TPU v7x, 512 devices: a whole 4x4x16 slice. The times are simulated.
512 devices in a mesh: sp: 128 (over z, x, core), tp: 4 (over y).
Axes of the slice: x: 4, y: 4, z: 16, core: 2. Of those that a mesh axis runs over, the one named last changes fastest.
Arguments:
- tokens: bfloat16 [16384, 2048], P(('sp', 'tp')), may hold values from -6 to 6
- norm_gain: float32 [2048], replicated, may hold values from 0.1 to 1.9
- w_query: bfloat16 [2048, 512], P(None, 'tp'), may hold values from -0.125 to 0.125
- w_key: bfloat16 [2048, 512], P(None, 'tp'), may hold values from -0.125 to 0.125
- w_value: bfloat16 [2048, 512], P(None, 'tp'), may hold values from -0.125 to 0.125
- score_offset: float32 [8], P('tp'), may hold values from -13 to -3, as said below
- w_out: bfloat16 [512, 2048], P('tp'), may hold values from -0.25 to 0.25
Outputs:
- mixed: bfloat16 [16384, 2048], P(('sp', 'tp'))
Inputs may be any that keep to these rules, and one draw needn't show every extreme that they name: `score_offset`: one offset a head.
All inputs are finite; a program needn't handle non-finite values.
Results may differ from a plain program's by a relative error of at most 0.01.
Values may be sent and summed in bfloat16 or wider, within the bound.
A program may use at most 64 MiB of HBM per device.

v0:
```python
import math

import jax
import jax.numpy as jnp
from jax import lax
from jax.sharding import Mesh
from jax.sharding import PartitionSpec as P

HEAD_DIM = 64
SP = ("sp_0", "sp_1", "sp_2")
SP_TP = ("sp_0", "sp_1", "sp_2", "tp")


RMS_EPS = 1e-06


def in_order(tiles, dim):
    tiles = jnp.moveaxis(tiles, 0, dim)
    dims = tiles.shape
    return tiles.reshape(*dims[:dim], dims[dim] * dims[dim + 1], *dims[dim + 2 :])


def sent_to_all(array, axis):
    copies = jnp.broadcast_to(array, (lax.axis_size(axis), *array.shape))
    return lax.all_to_all(copies, axis, split_axis=0, concat_axis=0, tiled=True)


def collect(array, axis, dim):
    return in_order(sent_to_all(array, axis), dim)


def gather_in_order(array, axes, sequence):
    tiles = array[None]
    for k in sequence:
        tiles = lax.all_gather(tiles, axes[k], axis=0, tiled=True)
    block = [lax.axis_size(axes[k]) for k in reversed(sequence)]
    tiles = tiles.reshape(*block, *array.shape)
    turned = sorted(range(len(sequence)), key=lambda place: sequence[len(sequence) - 1 - place])
    return tiles.transpose(*turned, *range(len(sequence), tiles.ndim)).reshape(-1, *array.shape)


def gather_axes(array, axes, sequence, dim):
    return in_order(gather_in_order(array, axes, sequence), dim)


def cut_along(array, dim, count):
    dims = array.shape
    tiles = array.reshape(*dims[:dim], count, dims[dim] // count, *dims[dim + 1 :])
    return jnp.moveaxis(tiles, dim, 0)


def sent_and_summed(array, axis, dim):
    tiles = cut_along(array, dim, lax.axis_size(axis))
    arrived = lax.all_to_all(tiles, axis, split_axis=0, concat_axis=0, tiled=True)
    return arrived.astype(jnp.float32).sum(axis=0)


def per_device(tokens, norm_gain, w_query, w_key, w_value, score_offset, w_out):
    groups = lax.axis_size("tp")
    tok_rows = tokens.shape[0] * groups
    head_width = w_query.shape[1]
    heads_dev = score_offset.shape[0]
    rows_f32 = collect(tokens, "tp", 0).astype(jnp.float32)
    inv_rms = lax.rsqrt(jnp.mean(rows_f32 * rows_f32, axis=1, keepdims=True) + RMS_EPS)
    normed = (rows_f32 * inv_rms * norm_gain).astype(jnp.bfloat16)
    projected = jnp.concatenate(
        [
            jnp.dot(normed, w_query, preferred_element_type=jnp.float32),
            jnp.dot(normed, w_key, preferred_element_type=jnp.float32),
            jnp.dot(normed, w_value, preferred_element_type=jnp.float32),
        ],
        axis=1,
    ).astype(jnp.bfloat16)
    queries = projected[:, :head_width].reshape(tok_rows, heads_dev, HEAD_DIM)
    key_vals = jnp.stack(
        [projected[:, head_width : 2 * head_width], projected[:, 2 * head_width :]]
    )
    own_index = lax.axis_index(SP)
    query_pos = own_index * tok_rows + jnp.arange(tok_rows, dtype=jnp.int32)
    offsets = score_offset[:, None, None]

    def absorb(running, key_block, key_start):
        totals, log_kept = running
        key_rows = key_block.shape[1]
        key_part = key_block[0].reshape(key_rows, heads_dev, HEAD_DIM)
        value_part = key_block[1].reshape(key_rows, heads_dev, HEAD_DIM)
        key_pos = key_start + jnp.arange(key_rows, dtype=jnp.int32)
        scores = (
            jnp.einsum("qhd,khd->hqk", queries, key_part, preferred_element_type=jnp.float32)
            * HEAD_DIM ** (-0.5)
            + offsets
        )
        earlier = ((key_pos[None, :] < query_pos[:, None]) & (key_pos[None, :] >= 0))[None]
        log_keep = jnp.where(earlier, jax.nn.log_sigmoid(-scores), 0.0)
        suffix = lax.cumsum(log_keep, axis=2, reverse=True) - log_keep + log_kept[:, :, None]
        weights = jnp.where(earlier, jnp.exp(jax.nn.log_sigmoid(scores) + suffix), 0.0).astype(
            jnp.bfloat16
        )
        totals = totals + jnp.einsum(
            "hqk,khd->hqd", weights, value_part, preferred_element_type=jnp.float32
        )
        return (totals, log_kept + jnp.sum(log_keep, axis=2))

    start_state = (
        jnp.zeros((heads_dev, tok_rows, HEAD_DIM), jnp.float32),
        jnp.zeros((heads_dev, tok_rows), jnp.float32),
    )
    all_keys = gather_axes(key_vals, SP, (1, 0, 2), 1)
    total_rows = all_keys.shape[1]
    span_rows = math.gcd(total_rows, 2048)
    span_count = total_rows // span_rows

    def sweep(turn_idx, carried):
        span_start = ((span_count - 1 - turn_idx) * span_rows).astype(jnp.int32)
        key_block = lax.dynamic_slice_in_dim(all_keys, span_start, span_rows, 1)
        return absorb(carried, key_block, span_start)

    finished = lax.fori_loop(0, span_count, sweep, start_state)
    mixed_rows = finished[0].transpose(1, 0, 2).reshape(tok_rows, head_width).astype(jnp.bfloat16)
    return sent_and_summed(
        jnp.dot(mixed_rows, w_out, preferred_element_type=jnp.float32).astype(jnp.bfloat16), "tp", 0
    ).astype(jnp.bfloat16)


def solution(mesh):
    finer = Mesh(mesh.devices.reshape(16, 4, 2, mesh.shape["tp"]), ("sp_0", "sp_1", "sp_2", "tp"))
    placed = (
        P(SP_TP, None),
        P(),
        P(None, "tp"),
        P(None, "tp"),
        P(None, "tp"),
        P("tp"),
        P("tp", None),
    )
    return jax.shard_map(
        per_device, mesh=finer, in_specs=placed, out_specs=P(SP_TP, None), check_vma=False
    )
```

profile of v0, /device:TPU:1, one launch (start us, length us, event | category | flops | bytes accessed | tf_op | source)
XLA Modules:
  0.0 320.8 jit_solution(11479637697951911001)
XLA Ops:
  6.6 1.1 broadcast_in_dim.56
  7.7 11.7 %all_to_all.10 = bf16[4,32,2048]{2,1,0:T(8,128)(2,1)S(1)} all-to-all(bf16[4,32,2048]{2,1,0:T(8,128)(2,1)S(1)} %broadcast_in_dim.56), channel_id=1, replica_groups=mesh['sp_0'=16,'sp_1'=4,'sp_2'=2,'tp'=4] {'tp'}, dimensions={0} | all-to-all | bytes 1048576 | tf_op jit(solution)/shard_map/all_to_all | solution.py:25
  20.5 12.1 %all-gather = bf16[8,128,128]{2,1,0:T(8,128)(2,1)} all-gather(bf16[2,128,128]{2,1,0:T(8,128)(2,1)S(1)} %pad_maximum_fusion), channel_id=2, replica_groups=mesh['sp_0'=16,'sp_1'=4,'sp_2'=2,'tp'=4] {'sp_1'}, dimensions={0}, use_global_device_ids=true | all-gather | bytes 327680 | tf_op jit(solution)/shard_map/all_gather | solution.py:35
  32.7 75.2 %all-gather.4.cloned.1.call-done = bf16[64,2,128,128]{3,2,1,0:T(8,128)(2,1)} async-done(((bf16[4,2,128,128]{3,2,1,0:T(8,128)(2,1)}), bf16[64,2,128,128]{3,2,1,0:T(8,128)(2,1)}) %all-gather.4.cloned.1.call-update) | async-done | bytes 4194320 | tf_op jit(solution)/shard_map/all_gather | solution.py:35
  108.0 1.0 copy-done.4
  109.3 37.7 %all-gather.6.cloned.1.call-done = bf16[128,2,128,128]{3,2,1,0:T(8,128)(2,1)} async-done(((bf16[64,2,128,128]{3,2,1,0:T(8,128)(2,1)}), bf16[128,2,128,128]{3,2,1,0:T(8,128)(2,1)}) %all-gather.6.cloned.1.call-update) | async-done | bytes 8388624 | tf_op jit(solution)/shard_map/all_gather | solution.py:35
  147.0 10.3 %copy.27 = bf16[16,4,2,2,128,128]{5,4,3,2,1,0:T(8,128)(2,1)} copy(bf16[16,4,2,2,128,128]{5,4,3,1,0,2:T(8,128)(2,1)} %bitcast.75) | data formatting | bytes 16777216 | tf_op jit(solution)/shard_map/transpose | solution.py:39
  157.3 10.3 %copy.28 = bf16[2,128,128,128]{3,2,1,0:T(8,128)(2,1)} copy(bf16[2,128,128,128]{3,2,0,1:T(8,128)(2,1)} %bitcast.72) | data formatting | bytes 16777216 | tf_op jit(solution)/shard_map/transpose | solution.py:18
  167.7 133.3 %while.16 = (s32[]{:T(128)}, f32[2,128,64]{1,2,0:T(8,128)S(1)}, f32[2,128]{1,0:T(2,128)S(1)}, bf16[2,16384,128]{2,1,0:T(8,128)(2,1)}, bf16[128,2,64]{0,2,1:T(8,1...) while((s32[]{:T(128)}, f32[2,128,64]{1,2,0:T(8,128)S(1)}, ...), condition=%wide.region_5.6_spmd.clone, body=%wide.region_1.5_spmd.clone.sunk | while | flops 218732672 | bytes 37794140 | solution.py:118
  167.7 1.5 compare_and_fusion.2
  169.2 1.3 constant_dynamic-slice_fusion.3
  170.9 3.2 fusion.46
  174.1 5.0 %fusion.47 = f32[2,128,16,128]{1,2,3,0:T(8,128)S(1)} fusion(f32[2,128,16,128]{1,3,2,0:T(8,128)S(1)} %bitcast.70), kind=kOutput, calls=%fused_computation.15.clone.1 | output fusion | flops 66584576 | bytes 4194304 | tf_op jit(solution)/shard_map/reduce-window.4
  179.4 0.6 copy.43
  180.0 1.0 copy-done.1
  181.0 3.0 fusion.49
  184.4 1.5 compare_and_fusion.2
  185.8 1.3 constant_dynamic-slice_fusion.3
  187.6 3.2 fusion.46
  190.8 5.0 %fusion.47 = f32[2,128,16,128]{1,2,3,0:T(8,128)S(1)} fusion(f32[2,128,16,128]{1,3,2,0:T(8,128)S(1)} %bitcast.70), kind=kOutput, calls=%fused_computation.15.clone.1 | output fusion | flops 66584576 | bytes 4194304 | tf_op jit(solution)/shard_map/reduce-window.4
  196.1 0.6 copy.43
  196.7 1.0 copy-done.1
  197.6 3.0 fusion.49
  201.0 1.5 compare_and_fusion.2
  202.5 1.3 constant_dynamic-slice_fusion.3
  204.2 3.2 fusion.46
  207.4 5.0 %fusion.47 = f32[2,128,16,128]{1,2,3,0:T(8,128)S(1)} fusion(f32[2,128,16,128]{1,3,2,0:T(8,128)S(1)} %bitcast.70), kind=kOutput, calls=%fused_computation.15.clone.1 | output fusion | flops 66584576 | bytes 4194304 | tf_op jit(solution)/shard_map/reduce-window.4
  212.7 0.6 copy.43
  213.4 1.0 copy-done.1
  214.3 3.0 fusion.49
  217.7 1.5 compare_and_fusion.2
  219.2 1.3 constant_dynamic-slice_fusion.3
  220.9 3.2 fusion.46
  224.1 5.0 %fusion.47 = f32[2,128,16,128]{1,2,3,0:T(8,128)S(1)} fusion(f32[2,128,16,128]{1,3,2,0:T(8,128)S(1)} %bitcast.70), kind=kOutput, calls=%fused_computation.15.clone.1 | output fusion | flops 66584576 | bytes 4194304 | tf_op jit(solution)/shard_map/reduce-window.4
  229.4 0.6 copy.43
  230.0 1.0 copy-done.1
  231.0 3.0 fusion.49
  234.4 1.5 compare_and_fusion.2
  235.9 1.3 constant_dynamic-slice_fusion.3
  237.6 3.2 fusion.46
  240.8 5.0 %fusion.47 = f32[2,128,16,128]{1,2,3,0:T(8,128)S(1)} fusion(f32[2,128,16,128]{1,3,2,0:T(8,128)S(1)} %bitcast.70), kind=kOutput, calls=%fused_computation.15.clone.1 | output fusion | flops 66584576 | bytes 4194304 | tf_op jit(solution)/shard_map/reduce-window.4
  246.1 0.6 copy.43
  246.7 1.0 copy-done.1
  247.7 3.0 fusion.49
  251.1 1.5 compare_and_fusion.2
  252.5 1.3 constant_dynamic-slice_fusion.3
  254.3 3.2 fusion.46
  257.4 5.0 %fusion.47 = f32[2,128,16,128]{1,2,3,0:T(8,128)S(1)} fusion(f32[2,128,16,128]{1,3,2,0:T(8,128)S(1)} %bitcast.70), kind=kOutput, calls=%fused_computation.15.clone.1 | output fusion | flops 66584576 | bytes 4194304 | tf_op jit(solution)/shard_map/reduce-window.4
  263.4 1.0 copy-done.1
  264.3 3.0 fusion.49
  267.7 1.5 compare_and_fusion.2
  269.2 1.3 constant_dynamic-slice_fusion.3
  270.9 3.2 fusion.46
  274.1 5.0 %fusion.47 = f32[2,128,16,128]{1,2,3,0:T(8,128)S(1)} fusion(f32[2,128,16,128]{1,3,2,0:T(8,128)S(1)} %bitcast.70), kind=kOutput, calls=%fused_computation.15.clone.1 | output fusion | flops 66584576 | bytes 4194304 | tf_op jit(solution)/shard_map/reduce-window.4
  280.1 1.0 copy-done.1
  281.0 3.0 fusion.49
  284.4 1.5 compare_and_fusion.2
  285.9 1.3 constant_dynamic-slice_fusion.3
  287.6 3.2 fusion.46
  290.8 5.0 %fusion.47 = f32[2,128,16,128]{1,2,3,0:T(8,128)S(1)} fusion(f32[2,128,16,128]{1,3,2,0:T(8,128)S(1)} %bitcast.70), kind=kOutput, calls=%fused_computation.15.clone.1 | output fusion | flops 66584576 | bytes 4194304 | tf_op jit(solution)/shard_map/reduce-window.4
  296.7 1.0 copy-done.1
  297.7 3.0 fusion.49
  301.4 11.9 %all_to_all.11 = bf16[4,32,2048]{2,1,0:T(8,128)(2,1)S(1)} all-to-all(bf16[4,32,2048]{2,1,0:T(8,128)(2,1)S(1)} %bitcast.76), channel_id=1, replica_groups=mesh['sp_0'=16,'sp_1'=4,'sp_2'=2,'tp'=4] {'tp'}, dimensions={0} | all-to-all | bytes 1048576 | tf_op jit(solution)/shard_map/all_to_all | solution.py:54
  313.2 0.7 reduce_sum.35
  (142 shorter events, 11.8 us)
Async XLA Ops:
  6.5 294.5 %copy-start = (bf16[128,2048]{1,0:T(8,128)(2,1)S(1)}, bf16[128,2048]{1,0:T(8,128)(2,1)}, u32[]{:S(2)}) copy-start(bf16[128,2048]{1,0:T(8,128)(2,1)} %param.15) | copy-start | bytes 1572868
  6.5 13.1 %copy-start.5 = (f32[2048]{0:T(1024)S(1)}, f32[2048]{0:T(1024)}, u32[]{:S(2)}) copy-start(f32[2048]{0:T(1024)} %param.10) | copy-start | bytes 24580
  6.5 13.3 %copy-start.2 = (bf16[2048,128]{1,0:T(8,128)(2,1)S(1)}, bf16[2048,128]{1,0:T(8,128)(2,1)}, u32[]{:S(2)}) copy-start(bf16[2048,128]{1,0:T(8,128)(2,1)} %param.13) | copy-start | bytes 1572868
  6.5 13.6 %copy-start.3 = (bf16[2048,128]{1,0:T(8,128)(2,1)S(1)}, bf16[2048,128]{1,0:T(8,128)(2,1)}, u32[]{:S(2)}) copy-start(bf16[2048,128]{1,0:T(8,128)(2,1)} %param.12) | copy-start | bytes 1572868
  6.5 101.4 %all-gather.4.cloned.1.call-start = ((), (), s32[]{:S(2)}) async-start(), calls=%async_computation.2 | async-start | bytes 4456448 | tf_op jit(solution)/shard_map/all_gather | solution.py:35
  32.7 114.3 %all-gather.6.cloned.1.call-start = ((), (), s32[]{:S(2)}) async-start(), calls=%async_computation.3 | async-start | bytes 12582912 | tf_op jit(solution)/shard_map/all_gather | solution.py:35
  107.9 1.0 copy-start.4
  157.3 10.4 %copy-start.6 = (f32[2]{0:T(128)S(1)}, f32[2]{0:T(128)}, u32[]{:S(2)}) copy-start(f32[2]{0:T(128)} %param.14) | copy-start | bytes 28
  179.4 1.6 copy-start.1
  181.0 3.3 %copy-start.7 = (f32[2]{0:T(128)S(1)}, f32[2]{0:T(128)}, u32[]{:S(2)}) copy-start(f32[2]{0:T(128)} %get-tuple-element.313) | copy-start | bytes 28 | tf_op jit(solution)/shard_map/while
  196.0 1.6 copy-start.1
  197.6 3.3 %copy-start.7 = (f32[2]{0:T(128)S(1)}, f32[2]{0:T(128)}, u32[]{:S(2)}) copy-start(f32[2]{0:T(128)} %get-tuple-element.313) | copy-start | bytes 28 | tf_op jit(solution)/shard_map/while
  212.7 1.6 copy-start.1
  214.3 3.3 %copy-start.7 = (f32[2]{0:T(128)S(1)}, f32[2]{0:T(128)}, u32[]{:S(2)}) copy-start(f32[2]{0:T(128)} %get-tuple-element.313) | copy-start | bytes 28 | tf_op jit(solution)/shard_map/while
  229.4 1.6 copy-start.1
  231.0 3.3 %copy-start.7 = (f32[2]{0:T(128)S(1)}, f32[2]{0:T(128)}, u32[]{:S(2)}) copy-start(f32[2]{0:T(128)} %get-tuple-element.313) | copy-start | bytes 28 | tf_op jit(solution)/shard_map/while
  246.1 1.6 copy-start.1
  247.7 3.3 %copy-start.7 = (f32[2]{0:T(128)S(1)}, f32[2]{0:T(128)}, u32[]{:S(2)}) copy-start(f32[2]{0:T(128)} %get-tuple-element.313) | copy-start | bytes 28 | tf_op jit(solution)/shard_map/while
  262.7 1.6 copy-start.1
  264.3 3.3 %copy-start.7 = (f32[2]{0:T(128)S(1)}, f32[2]{0:T(128)}, u32[]{:S(2)}) copy-start(f32[2]{0:T(128)} %get-tuple-element.313) | copy-start | bytes 28 | tf_op jit(solution)/shard_map/while
  279.4 1.6 copy-start.1
  281.0 3.3 %copy-start.7 = (f32[2]{0:T(128)S(1)}, f32[2]{0:T(128)}, u32[]{:S(2)}) copy-start(f32[2]{0:T(128)} %get-tuple-element.313) | copy-start | bytes 28 | tf_op jit(solution)/shard_map/while
  296.1 1.6 copy-start.1
  297.7 3.3 %copy-start.7 = (f32[2]{0:T(128)S(1)}, f32[2]{0:T(128)}, u32[]{:S(2)}) copy-start(f32[2]{0:T(128)} %get-tuple-element.313) | copy-start | bytes 28 | tf_op jit(solution)/shard_map/while
Sparse Core Ops, SparseCore 0:
  32.8 75.0 all-gather.3
  110.0 36.9 all-gather.5
where the time goes:
time: 322 us; the launch traced here: 321 us
  waiting for transfers between devices  113 us (35%)
  other arithmetic  79 us (25%)
  local copies, waits for them, and re-layouts  49.2 us (15%)
  blocking collectives  35.7 us (11%)
  matrix products  29.4 us (9%)
  between operations  13.5 us (4%)
    all_gather x2, waiting for transfers between devices, gather_in_order(): tiles = lax.all_gather(tiles, axes[k], axis=0, tiled=True)  113 us
    another operation x16, other arithmetic  40.8 us
    dot_general x8, matrix products, absorb(): jnp.einsum('qhd,khd->hqk', queries, key_part, preferred_element_type=jnp....  25.5 us
    convert_element_type x8, other arithmetic, absorb(): jnp.where(earlier, jnp.exp(jax.nn.log_sigmoid(scores) + suffix), 0.0)  23.9 us
    all_gather x1, blocking collectives, gather_in_order(): tiles = lax.all_gather(tiles, axes[k], axis=0, tiled=True)  12.1 us
    all_to_all x1, blocking collectives, sent_and_summed(): lax.all_to_all(tiles, axis, split_axis=0, concat_axis=0, tiled=True)  11.9 us
    and x8, other arithmetic, absorb(): (key_pos[None, :] < query_pos[:, None]) & (key_pos[None, :] >= 0)  11.8 us
    all_to_all x1, blocking collectives, sent_to_all(): return lax.all_to_all(copies, axis, split_axis=0, concat_axis=0, tiled=True)  11.7 us
  transfers between devices with their start and end apart: 2, of which 2 were waited for; matrix products, arithmetic and copies ran while one was open for 0% of the time, Pallas kernels for 0%

commit v1 on v0

v1 whole, which is shorter than its diff:
```python
import functools

import jax
import jax.numpy as jnp
from jax import lax
from jax.experimental import pallas as pl
from jax.experimental.pallas import tpu as pltpu
from jax.sharding import PartitionSpec as P

HEAD_DIM = 64
RMS_EPS = 1e-06
LOG2E = 1.4426950408889634
MESH = pl.DeviceIdType.MESH
NT = (((1,), (1,)), ((), ()))
NEG = -1e30
F32 = jnp.float32
BF16 = jnp.bfloat16


def dot(a, b):
    return jnp.dot(a, b, preferred_element_type=F32)


def layer_kernel(
    tok_ref, gain_ref, off_ref, wq_hbm, wk_hbm, wv_hbm, wo_hbm, out_ref,
    wq, wk, wv, wo_all, tok_all, normed, sib_out, sib_in, q_out, q_in, q_pad,
    kv_all, vt_all, z_s, l_s, part_o, part_s, o_out, s_out, o_in, s_in, acc_o, acc_s,
    att_out, att_in,
    sem_w, ysend, yrecv, y2send, y2recv, bsend, brecv, qsend, qrecv,
    zsend, zrecv, xsend, xrecv, x2send, x2recv, osend, orecv, ssend, srecv,
    wsend, wrecv, w2send, w2recv, asend, arecv,
):
    sp = lax.axis_index("sp")
    y = lax.axis_index("tp")
    z = sp // 8
    x = (sp // 2) % 4
    c = sp % 2
    group = z // 4
    r = z % 4

    def at(z_, x_, c_, y_):
        return ((z_ * 4 + x_) * 2 + c_, y_)

    def remote(src, dst, ss, rs, dev):
        return pltpu.make_async_remote_copy(
            src_ref=src, dst_ref=dst, send_sem=ss, recv_sem=rs, device_id=dev, device_id_type=MESH
        )

    loads = [
        pltpu.make_async_copy(wq_hbm, wq, sem_w.at[0]),
        pltpu.make_async_copy(wk_hbm, wk, sem_w.at[1]),
        pltpu.make_async_copy(wv_hbm, wv, sem_w.at[2]),
        pltpu.make_async_copy(wo_hbm, wo_all.at[y], sem_w.at[3]),
    ]
    for cp in loads:
        cp.start()

    y_up, y_dn, y_far = (y + 1) % 4, (y + 3) % 4, (y + 2) % 4
    peers = (at(z, x, c, y_up), at(z, x, c, y_dn))
    first = {}
    for h, d in ((0, 0), (1, 1), (1, 0), (0, 1)):
        cp = remote(tok_ref.at[h], tok_all.at[y, h], ysend.at[d, h], yrecv.at[d, h], peers[d])
        cp.start()
        first[d, h] = cp

    gain = gain_ref[...]

    def norm_rows(rows):
        rows = rows.astype(F32)
        inv = lax.rsqrt(jnp.mean(rows * rows, axis=1, keepdims=True) + RMS_EPS)
        return (rows * inv * gain).astype(BF16)

    for h in range(2):
        normed[y, pl.ds(h * 16, 16), :] = norm_rows(tok_ref[h])

    row_i = lax.broadcasted_iota(jnp.int32, (256, 256), 0)
    col_i = lax.broadcasted_iota(jnp.int32, (256, 256), 1)
    perm = jnp.where((row_i % 8) * 32 + row_i // 8 == col_i, 1.0, 0.0).astype(BF16)

    first[0, 0].wait_recv()
    relay0 = remote(tok_all.at[y_dn, 0], tok_all.at[y_dn, 0], y2send.at[0], y2recv.at[0], peers[0])
    relay0.start()
    first[1, 1].wait_recv()
    relay1 = remote(tok_all.at[y_up, 1], tok_all.at[y_up, 1], y2send.at[1], y2recv.at[1], peers[1])
    relay1.start()
    normed[y_dn, pl.ds(0, 16), :] = norm_rows(tok_all[y_dn, 0])
    normed[y_up, pl.ds(16, 16), :] = norm_rows(tok_all[y_up, 1])
    first[0, 1].wait_recv()
    normed[y_dn, pl.ds(16, 16), :] = norm_rows(tok_all[y_dn, 1])
    first[1, 0].wait_recv()
    normed[y_up, pl.ds(0, 16), :] = norm_rows(tok_all[y_up, 0])
    for cp in loads:
        cp.wait()
    relay0.wait_recv()
    normed[y_far, pl.ds(0, 16), :] = norm_rows(tok_all[y_far, 0])
    relay1.wait_recv()
    normed[y_far, pl.ds(16, 16), :] = norm_rows(tok_all[y_far, 1])

    rows = normed[...].reshape(128, 2048)
    q = dot(rows, wq[...])
    k = dot(rows, wk[...])
    v = dot(rows, wv[...])
    lane = lax.broadcasted_iota(jnp.int32, (128, 128), 1)
    low = lane < HEAD_DIM
    kv0 = jnp.where(low, k, pltpu.roll(v, HEAD_DIM, 1)).astype(BF16)
    kv1 = jnp.where(low, pltpu.roll(k, HEAD_DIM, 1), v).astype(BF16)
    mine0 = c == 0
    sib_out[0] = jnp.where(mine0, kv1, kv0)
    sib_out[1] = pltpu.roll(q, HEAD_DIM, 1).astype(BF16)
    sib = remote(sib_out, sib_in, bsend, brecv, at(z, x, 1 - c, y))
    sib.start()
    kv_mine = jnp.where(mine0, kv0, kv1)

    wo_sends = []
    for n, yy in enumerate((y_up, y_dn, y_far)):
        cp = remote(wo_all.at[y, c], wo_all.at[y, c], wsend.at[n], wrecv.at[n], at(z, x, c, yy))
        cp.start()
        wo_sends.append(cp)

    sib.wait_recv()
    q_first = (lane < HEAD_DIM) == mine0
    q_out[...] = jnp.where(q_first, q, sib_in[1].astype(F32)).astype(BF16)
    kv_sib = sib_in[0]
    pair = jnp.concatenate([jnp.where(mine0, kv_mine, kv_sib), jnp.where(mine0, kv_sib, kv_mine)], axis=0)
    kv_all[r, x] = dot(perm, pair).astype(BF16)

    def q_copy(n):
        return remote(q_out, q_in.at[n - 1], qsend.at[n - 1], qrecv.at[n - 1], at((z + 16 - 4 * n) % 16, x, c, y))

    def z_copy(n):
        return remote(
            kv_all.at[r, x], kv_all.at[r, x], zsend.at[n - 1], zrecv.at[n - 1],
            at(group * 4 + (r + n) % 4, x, c, y),
        )

    def x_copy(d, n):
        plane = (r + 4 - n) % 4
        return remote(
            kv_all.at[plane, x], kv_all.at[plane, x], xsend.at[d, n], xrecv.at[d, n],
            at(z, (x + (1 if d == 0 else 3)) % 4, c, y),
        )

    def x_relay(n):
        plane = (r + 4 - n) % 4
        d = 0 if n < 2 else 1
        src = (x + (3 if d == 0 else 1)) % 4
        return remote(
            kv_all.at[plane, src], kv_all.at[plane, src], x2send.at[n], x2recv.at[n],
            at(z, (x + (1 if d == 0 else 3)) % 4, c, y),
        )

    for n in (1, 3, 2):
        z_copy(n).start()
    for d in range(2):
        x_copy(d, 0).start()
    for n in (1, 2, 3):
        @pl.when(group >= n)
        def _():
            q_copy(n).start()

    def relay_step(n):
        d = 0 if n < 2 else 1
        x_copy(d, n).wait_recv()
        x_relay(n).start()

    def rest_step(n):
        d = 0 if n < 2 else 1
        x_copy(1 - d, n).wait_recv()
        x_relay(n).wait_recv()

    def pad_query(n, packed):
        packed = packed.astype(F32)
        q_pad[n, pl.ds(0, 128), :] = jnp.where(low, packed, 0.0).astype(BF16)
        q_pad[n, pl.ds(128, 128), :] = jnp.where(low, pltpu.roll(packed, HEAD_DIM, 1), 0.0).astype(BF16)

    pad_query(0, q_out[...])
    offset = off_ref[c] * LOG2E
    scale = HEAD_DIM ** (-0.5) * LOG2E
    sub = lax.broadcasted_iota(jnp.int32, (8, 256), 0)
    lane_q = lax.broadcasted_iota(jnp.int32, (32, 8, 256), 2)
    key_in = lax.broadcasted_iota(jnp.int32, (32, 8, 256), 1) * 32 + lax.broadcasted_iota(
        jnp.int32, (32, 8, 256), 0
    )

    def transpose_plane(plane):
        for b in range(4):
            vt_all[plane, :, pl.ds(b * 256, 256)] = (
                kv_all[plane, b].astype(F32).T[HEAD_DIM:, :].astype(BF16)
            )

    def item(n, plane, masked):
        qn = q_pad[n]
        sums = []
        for b in range(4):
            zz = lax.dot_general(kv_all[plane, b], qn, NT, preferred_element_type=F32)
            z2 = zz.reshape(32, 8, 256) * scale + offset
            if masked:
                z2 = jnp.where(key_in + b * 256 < lane_q + x * 256, z2, NEG)
            keep = jnp.maximum(z2, jnp.log2(1.0 + jnp.exp2(jnp.minimum(z2, 126.0))))
            z_s[b] = z2
            l_s[b] = keep
            sums.append(jnp.sum(keep, axis=0))
        later = jnp.zeros((1, 256), F32)
        for b in range(3, -1, -1):
            total = sums[b]
            incl = total
            for step in (1, 2, 4):
                moved = pltpu.roll(incl, 8 - step, 0)
                incl = incl + jnp.where(sub < 8 - step, moved, 0.0)
            run = incl - total + later
            later = later + incl[0:1]
            for i in range(31, -1, -1):
                run = run + l_s[b, i]
                z_s[b, i] = jnp.exp2(z_s[b, i] - run)
        w = z_s[...].reshape(1024, 256).astype(BF16)
        part_o[n, plane] = dot(vt_all[plane], w)
        part_s[n, plane] = jnp.broadcast_to(later, (8, 256))

    def blank(n, plane):
        part_o[n, plane] = jnp.zeros((HEAD_DIM, 256), F32)
        part_s[n, plane] = jnp.zeros((8, 256), F32)

    relay_step(0)
    for n in (1, 3, 2):
        z_copy(n).wait_recv()
        x_copy(0, n).start()
        x_copy(1, n).start()
    rest_step(0)
    transpose_plane(r)
    item(0, r, True)
    for n in (1, 3, 2):
        relay_step(n)
    for n in (1, 3, 2):
        rest_step(n)
        transpose_plane((r + 4 - n) % 4)

    def planes_of_own(n, _):
        plane = (r + 4 - n) % 4

        @pl.when(n <= r)
        def _():
            item(0, plane, False)

        @pl.when(n > r)
        def _():
            blank(0, plane)

        return 0

    lax.fori_loop(1, 4, planes_of_own, 0)

    def finish(n):
        o = part_o[n, 3]
        s = part_s[n, 3][0:1]
        for plane in (2, 1, 0):
            o = o + jnp.exp2(-s) * part_o[n, plane]
            s = s + part_s[n, plane][0:1]
        return o, s

    def o_copy(n):
        dev = at((z + 4 * n) % 16, x, c, y)
        return (
            remote(o_out.at[n - 1], o_in.at[n - 1], osend.at[n - 1], orecv.at[n - 1], dev),
            remote(s_out.at[n - 1], s_in.at[n - 1], ssend.at[n - 1], srecv.at[n - 1], dev),
        )

    for n in (3, 2, 1):
        @pl.when(group + n <= 3)
        def _():
            q_copy(n).wait_recv()
            pad_query(n, q_in[n - 1])

            def planes(plane, _):
                item(n, plane, False)
                return 0

            lax.fori_loop(0, 4, planes, 0)
            o, s = finish(n)
            o_out[n - 1] = o.astype(BF16)
            s_out[n - 1] = jnp.broadcast_to(s, (8, 256))
            for cp in o_copy(n):
                cp.start()

    wo_fwd = []
    for n, yy in enumerate((y_dn, y_up, y_far)):
        wo_sends[n].wait_recv()
        cp = remote(wo_all.at[yy, c], wo_all.at[yy, c], w2send.at[n], w2recv.at[n], at(z, x, 1 - c, y))
        cp.start()
        wo_fwd.append(cp)

    o, s = finish(0)
    acc_o[...] = o
    acc_s[...] = jnp.broadcast_to(s, (8, 256))
    for n in (1, 2, 3):
        @pl.when(group >= n)
        def _():
            for cp in o_copy(n):
                cp.wait_recv()
            s_ = acc_s[0:1, :]
            acc_o[...] += jnp.exp2(-s_) * o_in[n - 1].astype(F32)
            acc_s[...] += s_in[n - 1]

    o = acc_o[...]
    both = jnp.concatenate([jnp.where(mine0, o, 0.0), jnp.where(mine0, 0.0, o)], axis=0)
    att_out[...] = both.T.astype(BF16).reshape(8, 32, 128)
    a_sends = []
    for n in range(1, 8):
        cc = (c + n // 4) % 2
        yy = (y + n) % 4
        cp = remote(
            att_out.at[cc * 4 + yy], att_in.at[y * 2 + c], asend.at[n - 1], arecv.at[n - 1],
            at(z, x, cc, yy),
        )
        cp.start()
        a_sends.append(cp)
    att_in[y * 2 + c] = att_out[c * 4 + y]
    for cp in wo_fwd:
        cp.wait_recv()
    for cp in a_sends:
        cp.wait_recv()
    total = jnp.zeros((32, 2048), F32)
    for yy in range(4):
        feats = (att_in[2 * yy].astype(F32) + att_in[2 * yy + 1].astype(F32)).astype(BF16)
        part = dot(feats, wo_all[yy].reshape(128, 2048))
        total = total + part.astype(BF16).astype(F32)
    out_ref[...] = total.astype(BF16)

    for cp in first.values():
        cp.wait_send()
    relay0.wait_send()
    relay1.wait_send()
    sib.wait_send()
    for cp in wo_sends + wo_fwd + a_sends:
        cp.wait_send()
    for n in (1, 2, 3):
        z_copy(n).wait_send()

        @pl.when(group >= n)
        def _():
            q_copy(n).wait_send()

        @pl.when(group + n <= 3)
        def _():
            for cp in o_copy(n):
                cp.wait_send()

    for n in range(4):
        x_copy(0, n).wait_send()
        x_copy(1, n).wait_send()
        x_relay(n).wait_send()


def per_device(tokens, norm_gain, w_query, w_key, w_value, score_offset, w_out):
    vmem = pl.BlockSpec(memory_space=pltpu.VMEM)
    hbm = pl.BlockSpec(memory_space=pl.ANY)
    dma = pltpu.SemaphoreType.DMA
    v = pltpu.VMEM
    return pl.pallas_call(
        layer_kernel,
        out_shape=jax.ShapeDtypeStruct((32, 2048), BF16),
        in_specs=[vmem, vmem, pl.BlockSpec(memory_space=pltpu.SMEM), hbm, hbm, hbm, hbm],
        out_specs=vmem,
        scratch_shapes=[
            v((2048, 128), BF16), v((2048, 128), BF16), v((2048, 128), BF16), v((4, 2, 64, 2048), BF16),
            v((4, 2, 16, 2048), BF16), v((4, 32, 2048), BF16),
            v((2, 128, 128), BF16), v((2, 128, 128), BF16),
            v((128, 128), BF16), v((3, 128, 128), BF16), v((4, 256, 128), BF16),
            v((4, 4, 256, 128), BF16), v((4, HEAD_DIM, 1024), BF16),
            v((4, 32, 8, 256), F32), v((4, 32, 8, 256), F32),
            v((4, 4, HEAD_DIM, 256), F32), v((4, 4, 8, 256), F32),
            v((3, HEAD_DIM, 256), BF16), v((3, 8, 256), F32),
            v((3, HEAD_DIM, 256), BF16), v((3, 8, 256), F32),
            v((HEAD_DIM, 256), F32), v((8, 256), F32),
            v((8, 32, 128), BF16), v((8, 32, 128), BF16),
            dma((4,)), dma((2, 2)), dma((2, 2)), dma((2,)), dma((2,)), dma, dma, dma((3,)), dma((3,)),
            dma((3,)), dma((3,)), dma((2, 4)), dma((2, 4)), dma((4,)), dma((4,)),
            dma((3,)), dma((3,)), dma((3,)), dma((3,)),
            dma((3,)), dma((3,)), dma((3,)), dma((3,)), dma((7,)), dma((7,)),
        ],
        compiler_params=pltpu.CompilerParams(has_side_effects=True, vmem_limit_bytes=48 << 20),
    )(
        tokens.reshape(2, 16, 2048), norm_gain.reshape(1, 2048), score_offset,
        w_query, w_key, w_value, w_out.reshape(2, 64, 2048),
    )


def solution(mesh):
    rows = P(("sp", "tp"), None)
    placed = (rows, P(), P(None, "tp"), P(None, "tp"), P(None, "tp"), P("tp"), P("tp", None))
    return jax.shard_map(per_device, mesh=mesh, in_specs=placed, out_specs=rows, check_vma=False)
```

time: 322 us -> 73.9 us (0.23)
  the two profiles are of different devices: /device:TPU:1 before, /device:TPU:225 now
where the time goes in v1:
time: 73.9 us; the launch traced here: 73.5 us
  Pallas kernels  66.4 us (90%)
  local copies, waits for them, and re-layouts  7.08 us (10%)
    pallas_call x1, Pallas kernels, per_device(): pl.pallas_call(layer_kernel, out_shape=jax.ShapeDtypeStruct((32, 2048), B...  66.4 us
    unnamed x15, local copies, waits for them, and re-layouts  7.08 us

profile of v1, /device:TPU:225, one launch (start us, length us, event | category | flops | bytes accessed | tf_op | source)
XLA Modules:
  0.0 73.5 jit_solution(13763536904598805736)
XLA Ops:
  0.0 0.0 copy-start.6
  0.0 0.7 copy-done.6
  0.7 0.0 copy-start
  0.7 1.0 %copy-done = bf16[2048,128]{1,0:T(8,128)(2,1)S(1)} copy-done((bf16[2048,128]{1,0:T(8,128)(2,1)S(1)}, bf16[2048,128]{1,0:T(8,128)(2,1)}, u32[]{:S(2)}) %copy-start) | copy-done | bytes 524312
  1.7 0.0 copy-start.1
  1.7 1.0 %copy-done.1 = bf16[2048,128]{1,0:T(8,128)(2,1)S(1)} copy-done((bf16[2048,128]{1,0:T(8,128)(2,1)S(1)}, bf16[2048,128]{1,0:T(8,128)(2,1)}, u32[]{:S(2)}) %copy-start.1) | copy-done | bytes 524312
  2.7 0.0 copy-start.2
  2.7 1.0 %copy-done.2 = bf16[2048,128]{1,0:T(8,128)(2,1)S(1)} copy-done((bf16[2048,128]{1,0:T(8,128)(2,1)S(1)}, bf16[2048,128]{1,0:T(8,128)(2,1)}, u32[]{:S(2)}) %copy-start.2) | copy-done | bytes 524312
  3.8 0.0 copy-start.3
  3.8 1.0 %copy-done.3 = bf16[128,2048]{1,0:T(8,128)(2,1)S(1)} copy-done((bf16[128,2048]{1,0:T(8,128)(2,1)S(1)}, bf16[128,2048]{1,0:T(8,128)(2,1)}, u32[]{:S(2)}) %copy-start.3) | copy-done | bytes 524312
  4.8 0.0 copy-start.4
  4.8 0.9 %copy-done.4 = bf16[32,2048]{1,0:T(8,128)(2,1)S(1)} copy-done((bf16[32,2048]{1,0:T(8,128)(2,1)S(1)}, bf16[32,2048]{1,0:T(8,128)(2,1)}, u32[]{:S(2)}) %copy-start.4) | copy-done | bytes 131096
  5.7 0.0 copy-start.5
  5.7 0.7 copy-done.5
  6.4 66.4 %shard_map.73 = bf16[32,2048]{1,0:T(8,128)(2,1)S(1)} custom-call(bf16[2,16,2048]{2,1,0:T(8,128)(2,1)S(1)} %bitcast.4, f32[1,2048]{1,0:T(1,128)S(1)} %bitcast.5, f32[2]{0:T(128)S(1)} %copy-done.6, bf16[2048,128]{1,0:T(8,128)(2,1)S(1)} %copy-done, bf16[2048,128]{1,0:T(8,128)(2,1)S(1)} %copy-done.1, bf16[2048,128]{1,0:T(8,128)(2,1)S(1)} %copy-done.2, ...), custom_call_target="tpu_custom_call" | custom-call | tf_op jit(solution)/shard_map/pallas_call | solution.py:358
  72.9 0.7 copy.9
Async XLA Ops:
  0.0 0.7 copy-start.6
  0.7 1.0 %copy-start = (bf16[2048,128]{1,0:T(8,128)(2,1)S(1)}, bf16[2048,128]{1,0:T(8,128)(2,1)}, u32[]{:S(2)}) copy-start(bf16[2048,128]{1,0:T(8,128)(2,1)} %wq_hbm.1) | copy-start | bytes 1572868
  1.7 1.0 %copy-start.1 = (bf16[2048,128]{1,0:T(8,128)(2,1)S(1)}, bf16[2048,128]{1,0:T(8,128)(2,1)}, u32[]{:S(2)}) copy-start(bf16[2048,128]{1,0:T(8,128)(2,1)} %wk_hbm.1) | copy-start | bytes 1572868
  2.7 1.0 %copy-start.2 = (bf16[2048,128]{1,0:T(8,128)(2,1)S(1)}, bf16[2048,128]{1,0:T(8,128)(2,1)}, u32[]{:S(2)}) copy-start(bf16[2048,128]{1,0:T(8,128)(2,1)} %wv_hbm.1) | copy-start | bytes 1572868
  3.8 1.0 %copy-start.3 = (bf16[128,2048]{1,0:T(8,128)(2,1)S(1)}, bf16[128,2048]{1,0:T(8,128)(2,1)}, u32[]{:S(2)}) copy-start(bf16[128,2048]{1,0:T(8,128)(2,1)} %param.13) | copy-start | bytes 1572868
  4.8 0.9 %copy-start.4 = (bf16[32,2048]{1,0:T(8,128)(2,1)S(1)}, bf16[32,2048]{1,0:T(8,128)(2,1)}, u32[]{:S(2)}) copy-start(bf16[32,2048]{1,0:T(8,128)(2,1)} %param.7) | copy-start | bytes 393220
  5.7 0.7 copy-start.5

commit v2 on v1

--- a/solution.py
+++ b/solution.py
@@ -22,13 +22,13 @@
 
 
 def layer_kernel(
-    tok_ref, gain_ref, off_ref, wq_hbm, wk_hbm, wv_hbm, wo_hbm, out_ref,
-    wq, wk, wv, wo_all, tok_all, normed, sib_out, sib_in, q_out, q_in, q_pad,
-    kv_all, vt_all, z_s, l_s, part_o, part_s, o_out, s_out, o_in, s_in, acc_o, acc_s,
+    tok_hbm, gain_hbm, off_hbm, wq_hbm, wk_hbm, wv_hbm, wo_hbm, out_ref,
+    tok_ref, gain_ref, off_ref, wq, wk, wv, wo_all, tok_all, normed, sib_out, sib_in, q_out, q_in, q_pad,
+    kv_all, vt_all, e_s, l_s, w_s, part_o, part_s, o_out, s_out, o_in, s_in, acc_o, acc_s,
     att_out, att_in,
     sem_w, ysend, yrecv, y2send, y2recv, bsend, brecv, qsend, qrecv,
     zsend, zrecv, xsend, xrecv, x2send, x2recv, osend, orecv, ssend, srecv,
-    wsend, wrecv, w2send, w2recv, asend, arecv,
+    wsend, wrecv, w2send, w2recv, asend, arecv, hello,
 ):
     sp = lax.axis_index("sp")
     y = lax.axis_index("tp")
@@ -46,6 +46,13 @@
             src_ref=src, dst_ref=dst, send_sem=ss, recv_sem=rs, device_id=dev, device_id_type=MESH
         )
 
+    early = [
+        pltpu.make_async_copy(tok_hbm, tok_ref, sem_w.at[4]),
+        pltpu.make_async_copy(gain_hbm, gain_ref, sem_w.at[5]),
+        pltpu.make_async_copy(off_hbm, off_ref, sem_w.at[6]),
+    ]
+    for cp in early:
+        cp.start()
     loads = [
         pltpu.make_async_copy(wq_hbm, wq, sem_w.at[0]),
         pltpu.make_async_copy(wk_hbm, wk, sem_w.at[1]),
@@ -57,12 +64,27 @@
 
     y_up, y_dn, y_far = (y + 1) % 4, (y + 3) % 4, (y + 2) % 4
     peers = (at(z, x, c, y_up), at(z, x, c, y_dn))
+
+    def greet(sem, devs):
+        for dev in devs:
+            pl.semaphore_signal(sem, inc=1, device_id=dev, device_id_type=MESH)
+        pl.semaphore_wait(sem, len(devs))
+
+    def along_z(n):
+        return [at((z + n) % 16, x, c, y), at((z + 16 - n) % 16, x, c, y)]
+
+    partner = at(z, x, 1 - c, y)
+    sides = [at(z, (x + 1) % 4, c, y), at(z, (x + 3) % 4, c, y)]
+    greet(pltpu.get_barrier_semaphore(), [*peers, partner, *sides, *along_z(1)])
+    for cp in early:
+        cp.wait()
     first = {}
     for h, d in ((0, 0), (1, 1), (1, 0), (0, 1)):
         cp = remote(tok_ref.at[h], tok_all.at[y, h], ysend.at[d, h], yrecv.at[d, h], peers[d])
         cp.start()
         first[d, h] = cp
 
+    greet(hello.at[0], [*peers, partner, *along_z(1)])
     gain = gain_ref[...]
 
     def norm_rows(rows):
@@ -83,6 +105,10 @@
     first[1, 1].wait_recv()
     relay1 = remote(tok_all.at[y_up, 1], tok_all.at[y_up, 1], y2send.at[1], y2recv.at[1], peers[1])
     relay1.start()
+    greet(hello.at[1], [partner, *along_z(2)])
+    for dev in along_z(4):
+        pl.semaphore_signal(hello.at[2], inc=1, device_id=dev, device_id_type=MESH)
+    q_pad[...] = jnp.zeros((4, 256, 128), BF16)
     normed[y_dn, pl.ds(0, 16), :] = norm_rows(tok_all[y_dn, 0])
     normed[y_up, pl.ds(16, 16), :] = norm_rows(tok_all[y_up, 1])
     first[0, 1].wait_recv()
@@ -124,83 +150,85 @@
     pair = jnp.concatenate([jnp.where(mine0, kv_mine, kv_sib), jnp.where(mine0, kv_sib, kv_mine)], axis=0)
     kv_all[r, x] = dot(perm, pair).astype(BF16)
 
+    pl.semaphore_wait(hello.at[2], 2)
+
     def q_copy(n):
         return remote(q_out, q_in.at[n - 1], qsend.at[n - 1], qrecv.at[n - 1], at((z + 16 - 4 * n) % 16, x, c, y))
 
+    planes = (r, r + 1 - 2 * (r % 2), (r + 2) % 4, 3 - r)
+
     def z_copy(n):
         return remote(
-            kv_all.at[r, x], kv_all.at[r, x], zsend.at[n - 1], zrecv.at[n - 1],
-            at(group * 4 + (r + n) % 4, x, c, y),
+            kv_all.at[r, x], kv_all.at[r, x], zsend.at[n - 1], zrecv.at[n - 1], at(group * 4 + planes[n], x, c, y)
         )
 
     def x_copy(d, n):
-        plane = (r + 4 - n) % 4
-        return remote(
-            kv_all.at[plane, x], kv_all.at[plane, x], xsend.at[d, n], xrecv.at[d, n],
-            at(z, (x + (1 if d == 0 else 3)) % 4, c, y),
-        )
+        block = kv_all.at[planes[n], x]
+        return remote(block, block, xsend.at[d, n], xrecv.at[d, n], sides[d])
 
     def x_relay(n):
-        plane = (r + 4 - n) % 4
         d = 0 if n < 2 else 1
-        src = (x + (3 if d == 0 else 1)) % 4
-        return remote(
-            kv_all.at[plane, src], kv_all.at[plane, src], x2send.at[n], x2recv.at[n],
-            at(z, (x + (1 if d == 0 else 3)) % 4, c, y),
-        )
-
-    for n in (1, 3, 2):
-        z_copy(n).start()
-    for d in range(2):
-        x_copy(d, 0).start()
-    for n in (1, 2, 3):
-        @pl.when(group >= n)
-        def _():
-            q_copy(n).start()
-
-    def relay_step(n):
-        d = 0 if n < 2 else 1
-        x_copy(d, n).wait_recv()
+        block = kv_all.at[planes[n], (x + (3 if d == 0 else 1)) % 4]
+        return remote(block, block, x2send.at[n], x2recv.at[n], sides[d])
+
+    def spread(n):
+        if n:
+            z_copy(n).wait_recv()
+        x_copy(0, n).start()
+        x_copy(1, n).start()
+
+    def forward(n):
+        x_copy(0 if n < 2 else 1, n).wait_recv()
         x_relay(n).start()
 
-    def rest_step(n):
-        d = 0 if n < 2 else 1
-        x_copy(1 - d, n).wait_recv()
+    low_half = lane < HEAD_DIM
+
+    def complete(n):
+        x_copy(1 if n < 2 else 0, n).wait_recv()
         x_relay(n).wait_recv()
+        for b in range(4):
+            vt_all[planes[n], :, pl.ds(b * 256, 256)] = (
+                kv_all[planes[n], b].astype(F32).T[HEAD_DIM:, :].astype(BF16)
+            )
 
     def pad_query(n, packed):
         packed = packed.astype(F32)
-        q_pad[n, pl.ds(0, 128), :] = jnp.where(low, packed, 0.0).astype(BF16)
-        q_pad[n, pl.ds(128, 128), :] = jnp.where(low, pltpu.roll(packed, HEAD_DIM, 1), 0.0).astype(BF16)
-
-    pad_query(0, q_out[...])
+        q_pad[n, pl.ds(0, 128), :] = jnp.where(low_half, packed, 0.0).astype(BF16)
+        q_pad[n, pl.ds(128, 128), :] = jnp.where(low_half, pltpu.roll(packed, HEAD_DIM, 1), 0.0).astype(BF16)
+
+    def arrive(n):
+        @pl.when(group + n <= 3)
+        def _():
+            q_copy(n).wait_recv()
+            pad_query(n, q_in[n - 1])
+
     offset = off_ref[c] * LOG2E
     scale = HEAD_DIM ** (-0.5) * LOG2E
-    sub = lax.broadcasted_iota(jnp.int32, (8, 256), 0)
-    lane_q = lax.broadcasted_iota(jnp.int32, (32, 8, 256), 2)
-    key_in = lax.broadcasted_iota(jnp.int32, (32, 8, 256), 1) * 32 + lax.broadcasted_iota(
-        jnp.int32, (32, 8, 256), 0
-    )
-
-    def transpose_plane(plane):
-        for b in range(4):
-            vt_all[plane, :, pl.ds(b * 256, 256)] = (
-                kv_all[plane, b].astype(F32).T[HEAD_DIM:, :].astype(BF16)
-            )
-
-    def item(n, plane, masked):
-        qn = q_pad[n]
+    sub = lax.broadcasted_iota(jnp.int32, (8, 512), 0)
+    ahead = lax.broadcasted_iota(jnp.int32, (8, 256), 0) * 32 - lax.broadcasted_iota(jnp.int32, (8, 256), 1)
+
+    def block(first_n, plane):
         sums = []
         for b in range(4):
-            zz = lax.dot_general(kv_all[plane, b], qn, NT, preferred_element_type=F32)
-            z2 = zz.reshape(32, 8, 256) * scale + offset
-            if masked:
-                z2 = jnp.where(key_in + b * 256 < lane_q + x * 256, z2, NEG)
-            keep = jnp.maximum(z2, jnp.log2(1.0 + jnp.exp2(jnp.minimum(z2, 126.0))))
-            z_s[b] = z2
-            l_s[b] = keep
-            sums.append(jnp.sum(keep, axis=0))
-        later = jnp.zeros((1, 256), F32)
+            total = [None, None]
+            for h in range(2):
+                lanes = pl.ds(h * 256, 256)
+                zz = lax.dot_general(kv_all[plane, b], q_pad[first_n + h], NT, preferred_element_type=F32)
+                zz = zz.reshape(32, 8, 256)
+                limit = x * 256 - b * 256 + (r - plane) * 1024
+                for g in range(31, -1, -2):
+                    up = []
+                    for i in (g, g - 1):
+                        e = jnp.exp2(jnp.minimum(zz[i] * scale + offset, 60.0))
+                        if first_n + h == 0:
+                            e = jnp.where(ahead < limit - i, e, 0.0)
+                        e_s[b, i, :, lanes] = e
+                        up.append(1.0 + e)
+                    keep = jnp.log2(up[0] * up[1])
+                    l_s[b, g // 2, :, lanes] = keep
+                    total[h] = keep if total[h] is None else total[h] + keep
+            sums.append(jnp.concatenate(total, axis=1))
+        later = jnp.zeros((1, 512), F32)
         for b in range(3, -1, -1):
             total = sums[b]
             incl = total
@@ -209,45 +237,30 @@
                 incl = incl + jnp.where(sub < 8 - step, moved, 0.0)
             run = incl - total + later
             later = later + incl[0:1]
-            for i in range(31, -1, -1):
-                run = run + l_s[b, i]
-                z_s[b, i] = jnp.exp2(z_s[b, i] - run)
-        w = z_s[...].reshape(1024, 256).astype(BF16)
-        part_o[n, plane] = dot(vt_all[plane], w)
-        part_s[n, plane] = jnp.broadcast_to(later, (8, 256))
-
-    def blank(n, plane):
-        part_o[n, plane] = jnp.zeros((HEAD_DIM, 256), F32)
-        part_s[n, plane] = jnp.zeros((8, 256), F32)
-
-    relay_step(0)
-    for n in (1, 3, 2):
-        z_copy(n).wait_recv()
-        x_copy(0, n).start()
-        x_copy(1, n).start()
-    rest_step(0)
-    transpose_plane(r)
-    item(0, r, True)
-    for n in (1, 3, 2):
-        relay_step(n)
-    for n in (1, 3, 2):
-        rest_step(n)
-        transpose_plane((r + 4 - n) % 4)
-
-    def planes_of_own(n, _):
-        plane = (r + 4 - n) % 4
-
-        @pl.when(n <= r)
-        def _():
-            item(0, plane, False)
-
-        @pl.when(n > r)
-        def _():
-            blank(0, plane)
-
-        return 0
-
-    lax.fori_loop(1, 4, planes_of_own, 0)
+            for g in range(31, -1, -2):
+                run = run + l_s[b, g // 2]
+                left = jnp.exp2(-run)
+                e = e_s[b, g - 1]
+                w_s[b, g // 2] = jnp.concatenate([e * left, e_s[b, g] * (left * (1.0 + e))], axis=0).astype(BF16)
+        o = dot(vt_all[plane], w_s[...].reshape(1024, 512))
+        for h in range(2):
+            part_o[first_n + h, plane] = o[:, h * 256 : h * 256 + 256]
+            part_s[first_n + h, plane] = jnp.broadcast_to(later[:, h * 256 : h * 256 + 256], (8, 256))
+
+    def near(n):
+        @pl.when(jnp.logical_or(group < 3, planes[n] <= r))
+        def _():
+            block(0, planes[n])
+
+        @pl.when(jnp.logical_and(group == 3, planes[n] > r))
+        def _():
+            part_o[0, planes[n]] = jnp.zeros((HEAD_DIM, 256), F32)
+            part_s[0, planes[n]] = jnp.zeros((8, 256), F32)
+
+    def far(n):
+        @pl.when(group < 2)
+        def _():
+            block(2, planes[n])
 
     def finish(n):
         o = part_o[n, 3]
@@ -264,22 +277,49 @@
             remote(s_out.at[n - 1], s_in.at[n - 1], ssend.at[n - 1], srecv.at[n - 1], dev),
         )
 
-    for n in (3, 2, 1):
+    def give_back(n):
         @pl.when(group + n <= 3)
         def _():
-            q_copy(n).wait_recv()
-            pad_query(n, q_in[n - 1])
-
-            def planes(plane, _):
-                item(n, plane, False)
-                return 0
-
-            lax.fori_loop(0, 4, planes, 0)
             o, s = finish(n)
             o_out[n - 1] = o.astype(BF16)
             s_out[n - 1] = jnp.broadcast_to(s, (8, 256))
             for cp in o_copy(n):
                 cp.start()
+
+    spread(0)
+    z_copy(1).start()
+    for n in (2, 1, 3):
+        @pl.when(group >= n)
+        def _():
+            q_copy(n).start()
+    z_copy(2).start()
+    z_copy(3).start()
+    pad_query(0, q_out[...])
+    forward(0)
+    spread(1)
+    complete(0)
+    spread(2)
+    forward(1)
+    arrive(1)
+    near(0)
+    spread(3)
+    forward(2)
+    complete(1)
+    arrive(2)
+    arrive(3)
+    far(0)
+    near(1)
+    forward(3)
+    complete(2)
+    far(1)
+    near(2)
+    complete(3)
+    far(2)
+    far(3)
+    give_back(2)
+    give_back(3)
+    near(3)
+    give_back(1)
 
     wo_fwd = []
     for n, yy in enumerate((y_dn, y_up, y_far)):
@@ -351,33 +391,33 @@
 
 
 def per_device(tokens, norm_gain, w_query, w_key, w_value, score_offset, w_out):
-    vmem = pl.BlockSpec(memory_space=pltpu.VMEM)
     hbm = pl.BlockSpec(memory_space=pl.ANY)
     dma = pltpu.SemaphoreType.DMA
     v = pltpu.VMEM
     return pl.pallas_call(
         layer_kernel,
         out_shape=jax.ShapeDtypeStruct((32, 2048), BF16),
-        in_specs=[vmem, vmem, pl.BlockSpec(memory_space=pltpu.SMEM), hbm, hbm, hbm, hbm],
-        out_specs=vmem,
+        in_specs=[hbm] * 7,
+        out_specs=pl.BlockSpec(memory_space=pltpu.VMEM),
         scratch_shapes=[
+            v((2, 16, 2048), BF16), v((1, 2048), F32), pltpu.SMEM((2,), F32),
             v((2048, 128), BF16), v((2048, 128), BF16), v((2048, 128), BF16), v((4, 2, 64, 2048), BF16),
             v((4, 2, 16, 2048), BF16), v((4, 32, 2048), BF16),
             v((2, 128, 128), BF16), v((2, 128, 128), BF16),
             v((128, 128), BF16), v((3, 128, 128), BF16), v((4, 256, 128), BF16),
             v((4, 4, 256, 128), BF16), v((4, HEAD_DIM, 1024), BF16),
-            v((4, 32, 8, 256), F32), v((4, 32, 8, 256), F32),
+            v((4, 32, 8, 512), F32), v((4, 16, 8, 512), F32), v((4, 16, 16, 512), BF16),
             v((4, 4, HEAD_DIM, 256), F32), v((4, 4, 8, 256), F32),
             v((3, HEAD_DIM, 256), BF16), v((3, 8, 256), F32),
             v((3, HEAD_DIM, 256), BF16), v((3, 8, 256), F32),
             v((HEAD_DIM, 256), F32), v((8, 256), F32),
             v((8, 32, 128), BF16), v((8, 32, 128), BF16),
-            dma((4,)), dma((2, 2)), dma((2, 2)), dma((2,)), dma((2,)), dma, dma, dma((3,)), dma((3,)),
+            dma((7,)), dma((2, 2)), dma((2, 2)), dma((2,)), dma((2,)), dma, dma, dma((3,)), dma((3,)),
             dma((3,)), dma((3,)), dma((2, 4)), dma((2, 4)), dma((4,)), dma((4,)),
             dma((3,)), dma((3,)), dma((3,)), dma((3,)),
-            dma((3,)), dma((3,)), dma((3,)), dma((3,)), dma((7,)), dma((7,)),
+            dma((3,)), dma((3,)), dma((3,)), dma((3,)), dma((7,)), dma((7,)), pltpu.SemaphoreType.REGULAR((3,)),
         ],
-        compiler_params=pltpu.CompilerParams(has_side_effects=True, vmem_limit_bytes=48 << 20),
+        compiler_params=pltpu.CompilerParams(has_side_effects=True, collective_id=0, vmem_limit_bytes=67043328),
     )(
         tokens.reshape(2, 16, 2048), norm_gain.reshape(1, 2048), score_offset,
         w_query, w_key, w_value, w_out.reshape(2, 64, 2048),

time: 73.9 us -> 53.9 us (0.73)
  the two profiles are of different devices: /device:TPU:225 before, /device:TPU:1 now
where the time goes in v2:
time: 53.9 us; the launch traced here: 52.9 us
  Pallas kernels  51.3 us (95%)
  local copies, waits for them, and re-layouts  1.57 us (3%)
    pallas_call x1, Pallas kernels, per_device(): pl.pallas_call(layer_kernel, out_shape=jax.ShapeDtypeStruct((32, 2048), B...  51.3 us
    unnamed x1, local copies, waits for them, and re-layouts  1.57 us

profile of v2, /device:TPU:1, one launch (start us, length us, event | category | flops | bytes accessed | tf_op | source)
XLA Modules:
  0.0 52.9 jit_solution(17246018013039597204)
XLA Ops:
  0.0 51.3 %shard_map.73 = bf16[32,2048]{1,0:T(8,128)(2,1)} custom-call(bf16[2,16,2048]{2,1,0:T(8,128)(2,1)} %bitcast.4, f32[1,2048]{1,0:T(1,128)} %bitcast.5, f32[2]{0:T(128)} %off_hbm.1, bf16[2048,128]{1,0:T(8,128)(2,1)} %wq_hbm.1, bf16[2048,128]{1,0:T(8,128)(2,1)} %wk_hbm.1, bf16[2048,128]{1,0:T(8,128)(2,1)} %wv_hbm.1, bf16[2,64,2048]{2,1,0:T(8,128)(2,1)} %bitcast.3), custom_call_target="tpu_custom_call" | custom-call | tf_op jit(solution)/shard_map/pallas_call | solution.py:397
  51.3 1.6 %copy.9 = bf16[32,2048]{1,0:T(8,128)(2,1)} copy(bf16[32,2048]{1,0:T(8,128)(2,1)} %shard_map.73) | data formatting | bytes 262144

commit v3 on v2

--- a/solution.py
+++ b/solution.py
@@ -23,11 +23,11 @@
 
 def layer_kernel(
     tok_hbm, gain_hbm, off_hbm, wq_hbm, wk_hbm, wv_hbm, wo_hbm, out_ref,
-    tok_ref, gain_ref, off_ref, wq, wk, wv, wo_all, tok_all, normed, sib_out, sib_in, q_out, q_in, q_pad,
+    tok_ref, gain_ref, off_ref, w_qkv, wo_all, tok_all, normed, sib_out, sib_in, q_out, q_in, q_pad,
     kv_all, vt_all, e_s, l_s, w_s, part_o, part_s, o_out, s_out, o_in, s_in, acc_o, acc_s,
     att_out, att_in,
-    sem_w, ysend, yrecv, y2send, y2recv, bsend, brecv, qsend, qrecv,
-    zsend, zrecv, xsend, xrecv, x2send, x2recv, osend, orecv, ssend, srecv,
+    sem_w, ysend, yrecv, y2recv, bsend, brecv, qsend, qrecv,
+    zsend, zrecv, xsend, xrecv, x2recv, osend, orecv, ssend, srecv,
     wsend, wrecv, w2send, w2recv, asend, arecv, hello,
 ):
     sp = lax.axis_index("sp")
@@ -46,18 +46,21 @@
             src_ref=src, dst_ref=dst, send_sem=ss, recv_sem=rs, device_id=dev, device_id_type=MESH
         )
 
+    def settle(ref, sem):
+        pltpu.make_async_copy(ref, ref, sem).wait()
+
     early = [
-        pltpu.make_async_copy(tok_hbm, tok_ref, sem_w.at[4]),
-        pltpu.make_async_copy(gain_hbm, gain_ref, sem_w.at[5]),
-        pltpu.make_async_copy(off_hbm, off_ref, sem_w.at[6]),
+        pltpu.make_async_copy(tok_hbm, tok_ref, sem_w.at[2]),
+        pltpu.make_async_copy(gain_hbm, gain_ref, sem_w.at[3]),
+        pltpu.make_async_copy(off_hbm, off_ref, sem_w.at[4]),
     ]
     for cp in early:
         cp.start()
     loads = [
-        pltpu.make_async_copy(wq_hbm, wq, sem_w.at[0]),
-        pltpu.make_async_copy(wk_hbm, wk, sem_w.at[1]),
-        pltpu.make_async_copy(wv_hbm, wv, sem_w.at[2]),
-        pltpu.make_async_copy(wo_hbm, wo_all.at[y], sem_w.at[3]),
+        pltpu.make_async_copy(wq_hbm, w_qkv.at[0], sem_w.at[0]),
+        pltpu.make_async_copy(wk_hbm, w_qkv.at[1], sem_w.at[0]),
+        pltpu.make_async_copy(wv_hbm, w_qkv.at[2], sem_w.at[0]),
+        pltpu.make_async_copy(wo_hbm, wo_all.at[y], sem_w.at[1]),
     ]
     for cp in loads:
         cp.start()
@@ -80,7 +83,7 @@
         cp.wait()
     first = {}
     for h, d in ((0, 0), (1, 1), (1, 0), (0, 1)):
-        cp = remote(tok_ref.at[h], tok_all.at[y, h], ysend.at[d, h], yrecv.at[d, h], peers[d])
+        cp = remote(tok_ref.at[h], tok_all.at[y, h], ysend, yrecv.at[d, h], peers[d])
         cp.start()
         first[d, h] = cp
 
@@ -100,10 +103,10 @@
     perm = jnp.where((row_i % 8) * 32 + row_i // 8 == col_i, 1.0, 0.0).astype(BF16)
 
     first[0, 0].wait_recv()
-    relay0 = remote(tok_all.at[y_dn, 0], tok_all.at[y_dn, 0], y2send.at[0], y2recv.at[0], peers[0])
+    relay0 = remote(tok_all.at[y_dn, 0], tok_all.at[y_dn, 0], ysend, y2recv.at[0], peers[0])
     relay0.start()
     first[1, 1].wait_recv()
-    relay1 = remote(tok_all.at[y_up, 1], tok_all.at[y_up, 1], y2send.at[1], y2recv.at[1], peers[1])
+    relay1 = remote(tok_all.at[y_up, 1], tok_all.at[y_up, 1], ysend, y2recv.at[1], peers[1])
     relay1.start()
     greet(hello.at[1], [partner, *along_z(2)])
     for dev in along_z(4):
@@ -115,17 +118,17 @@
     normed[y_dn, pl.ds(16, 16), :] = norm_rows(tok_all[y_dn, 1])
     first[1, 0].wait_recv()
     normed[y_up, pl.ds(0, 16), :] = norm_rows(tok_all[y_up, 0])
-    for cp in loads:
-        cp.wait()
+    settle(w_qkv, sem_w.at[0])
+    loads[3].wait()
     relay0.wait_recv()
     normed[y_far, pl.ds(0, 16), :] = norm_rows(tok_all[y_far, 0])
     relay1.wait_recv()
     normed[y_far, pl.ds(16, 16), :] = norm_rows(tok_all[y_far, 1])
 
     rows = normed[...].reshape(128, 2048)
-    q = dot(rows, wq[...])
-    k = dot(rows, wk[...])
-    v = dot(rows, wv[...])
+    q = dot(rows, w_qkv[0])
+    k = dot(rows, w_qkv[1])
+    v = dot(rows, w_qkv[2])
     lane = lax.broadcasted_iota(jnp.int32, (128, 128), 1)
     low = lane < HEAD_DIM
     kv0 = jnp.where(low, k, pltpu.roll(v, HEAD_DIM, 1)).astype(BF16)
@@ -137,11 +140,9 @@
     sib.start()
     kv_mine = jnp.where(mine0, kv0, kv1)
 
-    wo_sends = []
-    for n, yy in enumerate((y_up, y_dn, y_far)):
-        cp = remote(wo_all.at[y, c], wo_all.at[y, c], wsend.at[n], wrecv.at[n], at(z, x, c, yy))
-        cp.start()
-        wo_sends.append(cp)
+    for yy in (y_up, y_dn, y_far):
+        remote(wo_all.at[y, c], wo_all.at[y, c], wsend, wrecv, at(z, x, c, yy)).start()
+    three_halves = wo_all.at[pl.ds(0, 3), 0]
 
     sib.wait_recv()
     q_first = (lane < HEAD_DIM) == mine0
@@ -150,26 +151,24 @@
     pair = jnp.concatenate([jnp.where(mine0, kv_mine, kv_sib), jnp.where(mine0, kv_sib, kv_mine)], axis=0)
     kv_all[r, x] = dot(perm, pair).astype(BF16)
 
-    pl.semaphore_wait(hello.at[2], 2)
-
     def q_copy(n):
-        return remote(q_out, q_in.at[n - 1], qsend.at[n - 1], qrecv.at[n - 1], at((z + 16 - 4 * n) % 16, x, c, y))
+        return remote(q_out, q_in.at[n - 1], qsend, qrecv.at[n - 1], at((z + 16 - 4 * n) % 16, x, c, y))
 
     planes = (r, r + 1 - 2 * (r % 2), (r + 2) % 4, 3 - r)
 
     def z_copy(n):
         return remote(
-            kv_all.at[r, x], kv_all.at[r, x], zsend.at[n - 1], zrecv.at[n - 1], at(group * 4 + planes[n], x, c, y)
+            kv_all.at[r, x], kv_all.at[r, x], zsend, zrecv.at[n - 1], at(group * 4 + planes[n], x, c, y)
         )
 
     def x_copy(d, n):
         block = kv_all.at[planes[n], x]
-        return remote(block, block, xsend.at[d, n], xrecv.at[d, n], sides[d])
+        return remote(block, block, xsend, xrecv.at[d, n], sides[d])
 
     def x_relay(n):
         d = 0 if n < 2 else 1
         block = kv_all.at[planes[n], (x + (3 if d == 0 else 1)) % 4]
-        return remote(block, block, x2send.at[n], x2recv.at[n], sides[d])
+        return remote(block, block, xsend, x2recv.at[n], sides[d])
 
     def spread(n):
         if n:
@@ -273,8 +272,8 @@
     def o_copy(n):
         dev = at((z + 4 * n) % 16, x, c, y)
         return (
-            remote(o_out.at[n - 1], o_in.at[n - 1], osend.at[n - 1], orecv.at[n - 1], dev),
-            remote(s_out.at[n - 1], s_in.at[n - 1], ssend.at[n - 1], srecv.at[n - 1], dev),
+            remote(o_out.at[n - 1], o_in.at[n - 1], osend, orecv.at[n - 1], dev),
+            remote(s_out.at[n - 1], s_in.at[n - 1], ssend, srecv.at[n - 1], dev),
         )
 
     def give_back(n):
@@ -286,30 +285,35 @@
             for cp in o_copy(n):
                 cp.start()
 
+    def ask(n):
+        @pl.when(group >= n)
+        def _():
+            q_copy(n).start()
+
     spread(0)
     z_copy(1).start()
-    for n in (2, 1, 3):
-        @pl.when(group >= n)
-        def _():
-            q_copy(n).start()
+    ask(1)
     z_copy(2).start()
     z_copy(3).start()
+    ask(3)
     pad_query(0, q_out[...])
     forward(0)
     spread(1)
+    pl.semaphore_wait(hello.at[2], 2)
+    ask(2)
+    spread(2)
     complete(0)
-    spread(2)
     forward(1)
+    spread(3)
     arrive(1)
     near(0)
-    spread(3)
     forward(2)
     complete(1)
+    near(1)
+    forward(3)
     arrive(2)
     arrive(3)
     far(0)
-    near(1)
-    forward(3)
     complete(2)
     far(1)
     near(2)
@@ -321,12 +325,9 @@
     near(3)
     give_back(1)
 
-    wo_fwd = []
-    for n, yy in enumerate((y_dn, y_up, y_far)):
-        wo_sends[n].wait_recv()
-        cp = remote(wo_all.at[yy, c], wo_all.at[yy, c], w2send.at[n], w2recv.at[n], at(z, x, 1 - c, y))
-        cp.start()
-        wo_fwd.append(cp)
+    settle(three_halves, wrecv)
+    for yy in (y_dn, y_up, y_far):
+        remote(wo_all.at[yy, c], wo_all.at[yy, c], w2send, w2recv, partner).start()
 
     o, s = finish(0)
     acc_o[...] = o
@@ -343,21 +344,13 @@
     o = acc_o[...]
     both = jnp.concatenate([jnp.where(mine0, o, 0.0), jnp.where(mine0, 0.0, o)], axis=0)
     att_out[...] = both.T.astype(BF16).reshape(8, 32, 128)
-    a_sends = []
     for n in range(1, 8):
         cc = (c + n // 4) % 2
         yy = (y + n) % 4
-        cp = remote(
-            att_out.at[cc * 4 + yy], att_in.at[y * 2 + c], asend.at[n - 1], arecv.at[n - 1],
-            at(z, x, cc, yy),
-        )
-        cp.start()
-        a_sends.append(cp)
+        remote(att_out.at[cc * 4 + yy], att_in.at[y * 2 + c], asend, arecv, at(z, x, cc, yy)).start()
     att_in[y * 2 + c] = att_out[c * 4 + y]
-    for cp in wo_fwd:
-        cp.wait_recv()
-    for cp in a_sends:
-        cp.wait_recv()
+    settle(three_halves, w2recv)
+    settle(att_in.at[pl.ds(0, 7)], arecv)
     total = jnp.zeros((32, 2048), F32)
     for yy in range(4):
         feats = (att_in[2 * yy].astype(F32) + att_in[2 * yy + 1].astype(F32)).astype(BF16)
@@ -365,29 +358,22 @@
         total = total + part.astype(BF16).astype(F32)
     out_ref[...] = total.astype(BF16)
 
-    for cp in first.values():
-        cp.wait_send()
-    relay0.wait_send()
-    relay1.wait_send()
+    settle(tok_all.at[pl.ds(0, 3)], ysend)
     sib.wait_send()
-    for cp in wo_sends + wo_fwd + a_sends:
-        cp.wait_send()
+    settle(three_halves, wsend)
+    settle(three_halves, w2send)
+    settle(att_out.at[pl.ds(0, 7)], asend)
+    settle(kv_all.at[0, pl.ds(0, 3)], zsend)
+    settle(kv_all.at[pl.ds(0, 3)], xsend)
     for n in (1, 2, 3):
-        z_copy(n).wait_send()
-
-        @pl.when(group >= n)
-        def _():
-            q_copy(n).wait_send()
-
-        @pl.when(group + n <= 3)
-        def _():
-            for cp in o_copy(n):
-                cp.wait_send()
-
-    for n in range(4):
-        x_copy(0, n).wait_send()
-        x_copy(1, n).wait_send()
-        x_relay(n).wait_send()
+        @pl.when(group == n)
+        def _():
+            settle(q_in.at[pl.ds(0, n)], qsend)
+
+        @pl.when(3 - group == n)
+        def _():
+            settle(o_in.at[pl.ds(0, n)], osend)
+            settle(s_in.at[pl.ds(0, n)], ssend)
 
 
 def per_device(tokens, norm_gain, w_query, w_key, w_value, score_offset, w_out):
@@ -401,7 +387,7 @@
         out_specs=pl.BlockSpec(memory_space=pltpu.VMEM),
         scratch_shapes=[
             v((2, 16, 2048), BF16), v((1, 2048), F32), pltpu.SMEM((2,), F32),
-            v((2048, 128), BF16), v((2048, 128), BF16), v((2048, 128), BF16), v((4, 2, 64, 2048), BF16),
+            v((3, 2048, 128), BF16), v((4, 2, 64, 2048), BF16),
             v((4, 2, 16, 2048), BF16), v((4, 32, 2048), BF16),
             v((2, 128, 128), BF16), v((2, 128, 128), BF16),
             v((128, 128), BF16), v((3, 128, 128), BF16), v((4, 256, 128), BF16),
@@ -412,10 +398,10 @@
             v((3, HEAD_DIM, 256), BF16), v((3, 8, 256), F32),
             v((HEAD_DIM, 256), F32), v((8, 256), F32),
             v((8, 32, 128), BF16), v((8, 32, 128), BF16),
-            dma((7,)), dma((2, 2)), dma((2, 2)), dma((2,)), dma((2,)), dma, dma, dma((3,)), dma((3,)),
-            dma((3,)), dma((3,)), dma((2, 4)), dma((2, 4)), dma((4,)), dma((4,)),
-            dma((3,)), dma((3,)), dma((3,)), dma((3,)),
-            dma((3,)), dma((3,)), dma((3,)), dma((3,)), dma((7,)), dma((7,)), pltpu.SemaphoreType.REGULAR((3,)),
+            dma((5,)), dma, dma((2, 2)), dma((2,)), dma, dma, dma, dma((3,)),
+            dma, dma((3,)), dma, dma((2, 4)), dma((4,)),
+            dma, dma((3,)), dma, dma((3,)),
+            dma, dma, dma, dma, dma, dma, pltpu.SemaphoreType.REGULAR((3,)),
         ],
         compiler_params=pltpu.CompilerParams(has_side_effects=True, collective_id=0, vmem_limit_bytes=67043328),
     )(

time: 53.9 us -> 52 us (0.965)
  the two profiles are of different devices: /device:TPU:1 before, /device:TPU:385 now
where the time goes in v3:
time: 52 us; the launch traced here: 51.9 us
  Pallas kernels  50.3 us (97%)
  local copies, waits for them, and re-layouts  1.57 us (3%)
    pallas_call x1, Pallas kernels, per_device(): pl.pallas_call(layer_kernel, out_shape=jax.ShapeDtypeStruct((32, 2048), B...  50.3 us
    unnamed x1, local copies, waits for them, and re-layouts  1.57 us

profile of v3, /device:TPU:385, one launch (start us, length us, event | category | flops | bytes accessed | tf_op | source)
XLA Modules:
  0.0 51.9 jit_solution(4087139095237883501)
XLA Ops:
  0.0 50.3 %shard_map.73 = bf16[32,2048]{1,0:T(8,128)(2,1)} custom-call(bf16[2,16,2048]{2,1,0:T(8,128)(2,1)} %bitcast.4, f32[1,2048]{1,0:T(1,128)} %bitcast.5, f32[2]{0:T(128)} %off_hbm.1, bf16[2048,128]{1,0:T(8,128)(2,1)} %wq_hbm.1, bf16[2048,128]{1,0:T(8,128)(2,1)} %wk_hbm.1, bf16[2048,128]{1,0:T(8,128)(2,1)} %wv_hbm.1, bf16[2,64,2048]{2,1,0:T(8,128)(2,1)} %bitcast.3), custom_call_target="tpu_custom_call" | custom-call | tf_op jit(solution)/shard_map/pallas_call | solution.py:383
  50.3 1.6 %copy.9 = bf16[32,2048]{1,0:T(8,128)(2,1)} copy(bf16[32,2048]{1,0:T(8,128)(2,1)} %shard_map.73) | data formatting | bytes 262144

commit v4 on v3

--- a/solution.py
+++ b/solution.py
@@ -203,23 +203,26 @@
 
     offset = off_ref[c] * LOG2E
     scale = HEAD_DIM ** (-0.5) * LOG2E
-    sub = lax.broadcasted_iota(jnp.int32, (8, 512), 0)
     ahead = lax.broadcasted_iota(jnp.int32, (8, 256), 0) * 32 - lax.broadcasted_iota(jnp.int32, (8, 256), 1)
 
-    def block(first_n, plane):
+    def block(*pairs):
+        pairs = [(n, planes[m]) for n, m in pairs]
+        wide = 256 * len(pairs)
+        every = pl.ds(0, wide)
+        sub = lax.broadcasted_iota(jnp.int32, (8, wide), 0)
         sums = []
         for b in range(4):
-            total = [None, None]
-            for h in range(2):
+            total = [None] * len(pairs)
+            for h, (n, plane) in enumerate(pairs):
                 lanes = pl.ds(h * 256, 256)
-                zz = lax.dot_general(kv_all[plane, b], q_pad[first_n + h], NT, preferred_element_type=F32)
+                zz = lax.dot_general(kv_all[plane, b], q_pad[n], NT, preferred_element_type=F32)
                 zz = zz.reshape(32, 8, 256)
                 limit = x * 256 - b * 256 + (r - plane) * 1024
                 for g in range(31, -1, -2):
                     up = []
                     for i in (g, g - 1):
                         e = jnp.exp2(jnp.minimum(zz[i] * scale + offset, 60.0))
-                        if first_n + h == 0:
+                        if n == 0:
                             e = jnp.where(ahead < limit - i, e, 0.0)
                         e_s[b, i, :, lanes] = e
                         up.append(1.0 + e)
@@ -227,7 +230,7 @@
                     l_s[b, g // 2, :, lanes] = keep
                     total[h] = keep if total[h] is None else total[h] + keep
             sums.append(jnp.concatenate(total, axis=1))
-        later = jnp.zeros((1, 512), F32)
+        later = jnp.zeros((1, wide), F32)
         for b in range(3, -1, -1):
             total = sums[b]
             incl = total
@@ -237,29 +240,40 @@
             run = incl - total + later
             later = later + incl[0:1]
             for g in range(31, -1, -2):
-                run = run + l_s[b, g // 2]
+                run = run + l_s[b, g // 2, :, every]
                 left = jnp.exp2(-run)
-                e = e_s[b, g - 1]
-                w_s[b, g // 2] = jnp.concatenate([e * left, e_s[b, g] * (left * (1.0 + e))], axis=0).astype(BF16)
-        o = dot(vt_all[plane], w_s[...].reshape(1024, 512))
-        for h in range(2):
-            part_o[first_n + h, plane] = o[:, h * 256 : h * 256 + 256]
-            part_s[first_n + h, plane] = jnp.broadcast_to(later[:, h * 256 : h * 256 + 256], (8, 256))
-
-    def near(n):
-        @pl.when(jnp.logical_or(group < 3, planes[n] <= r))
-        def _():
-            block(0, planes[n])
-
-        @pl.when(jnp.logical_and(group == 3, planes[n] > r))
+                e = e_s[b, g - 1, :, every]
+                w_s[b, g // 2, :, every] = jnp.concatenate(
+                    [e * left, e_s[b, g, :, every] * (left * (1.0 + e))], axis=0
+                ).astype(BF16)
+        for h, (n, plane) in enumerate(pairs):
+            part_o[n, plane] = dot(vt_all[plane], w_s[:, :, :, pl.ds(h * 256, 256)].reshape(1024, 256))
+            part_s[n, plane] = jnp.broadcast_to(later[:, h * 256 : h * 256 + 256], (8, 256))
+
+    def own(n):
+        @pl.when(planes[n] <= r)
+        def _():
+            block((0, n))
+
+        @pl.when(planes[n] > r)
         def _():
             part_o[0, planes[n]] = jnp.zeros((HEAD_DIM, 256), F32)
             part_s[0, planes[n]] = jnp.zeros((8, 256), F32)
 
-    def far(n):
+    def near_groups(first, *pairs):
+        @pl.when(jnp.logical_and(group >= first, group < 3))
+        def _():
+            block(*pairs)
+
+    def group_is(g, *pairs):
+        @pl.when(group == g)
+        def _():
+            block(*pairs)
+
+    def two_groups(*pairs):
         @pl.when(group < 2)
         def _():
-            block(2, planes[n])
+            block(*pairs)
 
     def finish(n):
         o = part_o[n, 3]
@@ -281,7 +295,7 @@
         def _():
             o, s = finish(n)
             o_out[n - 1] = o.astype(BF16)
-            s_out[n - 1] = jnp.broadcast_to(s, (8, 256))
+            s_out[n - 1] = s
             for cp in o_copy(n):
                 cp.start()
 
@@ -303,27 +317,32 @@
     ask(2)
     spread(2)
     complete(0)
+    spread(3)
     forward(1)
-    spread(3)
+    own(0)
+    forward(2)
     arrive(1)
-    near(0)
-    forward(2)
+    arrive(3)
+    group_is(0, (1, 0), (3, 0))
+    forward(3)
     complete(1)
-    near(1)
-    forward(3)
+    group_is(0, (1, 1), (3, 1))
+    near_groups(1, (1, 0), (1, 1))
     arrive(2)
-    arrive(3)
-    far(0)
     complete(2)
-    far(1)
-    near(2)
+    two_groups((2, 0), (2, 1), (2, 2))
     complete(3)
-    far(2)
-    far(3)
+    group_is(0, (2, 3), (1, 2), (3, 2))
+    group_is(1, (2, 3), (1, 2))
     give_back(2)
+    group_is(0, (1, 3), (3, 3))
     give_back(3)
-    near(3)
+    group_is(1, (1, 3))
+    group_is(2, (1, 2), (1, 3))
     give_back(1)
+    own(1)
+    own(2)
+    own(3)
 
     settle(three_halves, wrecv)
     for yy in (y_dn, y_up, y_far):
@@ -339,7 +358,7 @@
                 cp.wait_recv()
             s_ = acc_s[0:1, :]
             acc_o[...] += jnp.exp2(-s_) * o_in[n - 1].astype(F32)
-            acc_s[...] += s_in[n - 1]
+            acc_s[...] = jnp.broadcast_to(s_ + s_in[n - 1], (8, 256))
 
     o = acc_o[...]
     both = jnp.concatenate([jnp.where(mine0, o, 0.0), jnp.where(mine0, 0.0, o)], axis=0)
@@ -392,10 +411,10 @@
             v((2, 128, 128), BF16), v((2, 128, 128), BF16),
             v((128, 128), BF16), v((3, 128, 128), BF16), v((4, 256, 128), BF16),
             v((4, 4, 256, 128), BF16), v((4, HEAD_DIM, 1024), BF16),
-            v((4, 32, 8, 512), F32), v((4, 16, 8, 512), F32), v((4, 16, 16, 512), BF16),
+            v((4, 32, 8, 768), F32), v((4, 16, 8, 768), F32), v((4, 16, 16, 768), BF16),
             v((4, 4, HEAD_DIM, 256), F32), v((4, 4, 8, 256), F32),
-            v((3, HEAD_DIM, 256), BF16), v((3, 8, 256), F32),
-            v((3, HEAD_DIM, 256), BF16), v((3, 8, 256), F32),
+            v((3, HEAD_DIM, 256), BF16), v((3, 1, 256), F32),
+            v((3, HEAD_DIM, 256), BF16), v((3, 1, 256), F32),
             v((HEAD_DIM, 256), F32), v((8, 256), F32),
             v((8, 32, 128), BF16), v((8, 32, 128), BF16),
             dma((5,)), dma, dma((2, 2)), dma((2,)), dma, dma, dma, dma((3,)),

time: 52 us -> 49.8 us (0.958)
  the two profiles are of different devices: /device:TPU:385 before, /device:TPU:1 now
where the time goes in v4:
time: 49.8 us; the launch traced here: 48.9 us
  Pallas kernels  47.3 us (95%)
  local copies, waits for them, and re-layouts  1.57 us (3%)
    pallas_call x1, Pallas kernels, per_device(): pl.pallas_call(layer_kernel, out_shape=jax.ShapeDtypeStruct((32, 2048), B...  47.3 us
    unnamed x1, local copies, waits for them, and re-layouts  1.57 us

profile of v4, /device:TPU:1, one launch (start us, length us, event | category | flops | bytes accessed | tf_op | source)
XLA Modules:
  0.0 48.9 jit_solution(8806230119360954690)
XLA Ops:
  0.0 47.3 %shard_map.73 = bf16[32,2048]{1,0:T(8,128)(2,1)} custom-call(bf16[2,16,2048]{2,1,0:T(8,128)(2,1)} %bitcast.4, f32[1,2048]{1,0:T(1,128)} %bitcast.5, f32[2]{0:T(128)} %off_hbm.1, bf16[2048,128]{1,0:T(8,128)(2,1)} %wq_hbm.1, bf16[2048,128]{1,0:T(8,128)(2,1)} %wk_hbm.1, bf16[2048,128]{1,0:T(8,128)(2,1)} %wv_hbm.1, bf16[2,64,2048]{2,1,0:T(8,128)(2,1)} %bitcast.3), custom_call_target="tpu_custom_call" | custom-call | tf_op jit(solution)/shard_map/pallas_call | solution.py:402
  47.4 1.6 %copy.9 = bf16[32,2048]{1,0:T(8,128)(2,1)} copy(bf16[32,2048]{1,0:T(8,128)(2,1)} %shard_map.73) | data formatting | bytes 262144

commit v5 on v4

--- a/solution.py
+++ b/solution.py
@@ -81,13 +81,19 @@
     greet(pltpu.get_barrier_semaphore(), [*peers, partner, *sides, *along_z(1)])
     for cp in early:
         cp.wait()
+    cols = (pl.ds(0, 1024), pl.ds(1024, 1024))
     first = {}
-    for h, d in ((0, 0), (1, 1), (1, 0), (0, 1)):
-        cp = remote(tok_ref.at[h], tok_all.at[y, h], ysend, yrecv.at[d, h], peers[d])
+    for n in range(2):
+        for d in range(2):
+            first[d, n] = remote(
+                tok_ref.at[d, :, cols[n]], tok_all.at[y, d, :, cols[n]], ysend, yrecv.at[d, n], peers[d]
+            )
+    for d in range(2):
+        first[d, 2] = remote(tok_ref.at[1 - d], tok_all.at[y, 1 - d], ysend, yrecv.at[d, 2], peers[d])
+    for cp in first.values():
         cp.start()
-        first[d, h] = cp
-
-    greet(hello.at[0], [*peers, partner, *along_z(1)])
+
+    greet(hello.at[0], [*peers, partner, *sides, *along_z(1)])
     gain = gain_ref[...]
 
     def norm_rows(rows):
@@ -102,28 +108,29 @@
     col_i = lax.broadcasted_iota(jnp.int32, (256, 256), 1)
     perm = jnp.where((row_i % 8) * 32 + row_i // 8 == col_i, 1.0, 0.0).astype(BF16)
 
-    first[0, 0].wait_recv()
-    relay0 = remote(tok_all.at[y_dn, 0], tok_all.at[y_dn, 0], ysend, y2recv.at[0], peers[0])
-    relay0.start()
-    first[1, 1].wait_recv()
-    relay1 = remote(tok_all.at[y_up, 1], tok_all.at[y_up, 1], ysend, y2recv.at[1], peers[1])
-    relay1.start()
+    relays = []
+    for n in range(2):
+        for d in range(2):
+            first[d, n].wait_recv()
+            piece = tok_all.at[(y_dn, y_up)[d], d, :, cols[n]]
+            relays.append(remote(piece, piece, ysend, y2recv.at[d, n], peers[d]))
+            relays[-1].start()
     greet(hello.at[1], [partner, *along_z(2)])
     for dev in along_z(4):
         pl.semaphore_signal(hello.at[2], inc=1, device_id=dev, device_id_type=MESH)
     q_pad[...] = jnp.zeros((4, 256, 128), BF16)
     normed[y_dn, pl.ds(0, 16), :] = norm_rows(tok_all[y_dn, 0])
     normed[y_up, pl.ds(16, 16), :] = norm_rows(tok_all[y_up, 1])
-    first[0, 1].wait_recv()
+    first[0, 2].wait_recv()
     normed[y_dn, pl.ds(16, 16), :] = norm_rows(tok_all[y_dn, 1])
-    first[1, 0].wait_recv()
+    first[1, 2].wait_recv()
     normed[y_up, pl.ds(0, 16), :] = norm_rows(tok_all[y_up, 0])
     settle(w_qkv, sem_w.at[0])
     loads[3].wait()
-    relay0.wait_recv()
-    normed[y_far, pl.ds(0, 16), :] = norm_rows(tok_all[y_far, 0])
-    relay1.wait_recv()
-    normed[y_far, pl.ds(16, 16), :] = norm_rows(tok_all[y_far, 1])
+    for d in range(2):
+        relays[d].wait_recv()
+        relays[d + 2].wait_recv()
+        normed[y_far, pl.ds(16 * d, 16), :] = norm_rows(tok_all[y_far, d])
 
     rows = normed[...].reshape(128, 2048)
     q = dot(rows, w_qkv[0])
@@ -151,8 +158,11 @@
     pair = jnp.concatenate([jnp.where(mine0, kv_mine, kv_sib), jnp.where(mine0, kv_sib, kv_mine)], axis=0)
     kv_all[r, x] = dot(perm, pair).astype(BF16)
 
+    below = {1: (z + 12) % 16, 2: (z + 27 - 2 * r) % 16, 3: (z + 4) % 16}
+    above = {1: (z + 4) % 16, 2: (z + 27 - 2 * r) % 16, 3: (z + 12) % 16}
+
     def q_copy(n):
-        return remote(q_out, q_in.at[n - 1], qsend, qrecv.at[n - 1], at((z + 16 - 4 * n) % 16, x, c, y))
+        return remote(q_out, q_in.at[n - 1], qsend, qrecv.at[n - 1], at(below[n], x, c, y))
 
     planes = (r, r + 1 - 2 * (r % 2), (r + 2) % 4, 3 - r)
 
@@ -166,24 +176,30 @@
         return remote(block, block, xsend, xrecv.at[d, n], sides[d])
 
     def x_relay(n):
-        d = 0 if n < 2 else 1
-        block = kv_all.at[planes[n], (x + (3 if d == 0 else 1)) % 4]
-        return remote(block, block, xsend, x2recv.at[n], sides[d])
+        if n < 2:
+            block = kv_all.at[planes[n], (x + (3, 1)[n]) % 4]
+            return remote(block, block, xsend, x2recv.at[n], sides[n])
+        block = kv_all.at[planes[n], x]
+        return remote(block, block, xsend, x2recv.at[n], at(z, (x + 2) % 4, c, y))
 
     def spread(n):
         if n:
             z_copy(n).wait_recv()
         x_copy(0, n).start()
         x_copy(1, n).start()
+        if n >= 2:
+            x_relay(n).start()
 
     def forward(n):
-        x_copy(0 if n < 2 else 1, n).wait_recv()
+        x_copy(n, n).wait_recv()
         x_relay(n).start()
 
     low_half = lane < HEAD_DIM
 
     def complete(n):
-        x_copy(1 if n < 2 else 0, n).wait_recv()
+        for d in range(2):
+            if d != n:
+                x_copy(d, n).wait_recv()
         x_relay(n).wait_recv()
         for b in range(4):
             vt_all[planes[n], :, pl.ds(b * 256, 256)] = (
@@ -250,15 +266,17 @@
             part_o[n, plane] = dot(vt_all[plane], w_s[:, :, :, pl.ds(h * 256, 256)].reshape(1024, 256))
             part_s[n, plane] = jnp.broadcast_to(later[:, h * 256 : h * 256 + 256], (8, 256))
 
-    def own(n):
-        @pl.when(planes[n] <= r)
-        def _():
-            block((0, n))
-
-        @pl.when(planes[n] > r)
-        def _():
-            part_o[0, planes[n]] = jnp.zeros((HEAD_DIM, 256), F32)
-            part_s[0, planes[n]] = jnp.zeros((8, 256), F32)
+    for m in (1, 2, 3):
+        @pl.when(planes[m] > r)
+        def _():
+            part_o[0, planes[m]] = jnp.zeros((HEAD_DIM, 256), F32)
+            part_s[0, planes[m]] = jnp.zeros((8, 256), F32)
+
+    def own_rest():
+        for plane, pairs in ((1, ((0, 1),)), (2, ((0, 2), (0, 3))), (3, ((0, 1), (0, 2), (0, 3)))):
+            @pl.when(r == plane)
+            def _():
+                block(*pairs)
 
     def near_groups(first, *pairs):
         @pl.when(jnp.logical_and(group >= first, group < 3))
@@ -284,7 +302,7 @@
         return o, s
 
     def o_copy(n):
-        dev = at((z + 4 * n) % 16, x, c, y)
+        dev = at(above[n], x, c, y)
         return (
             remote(o_out.at[n - 1], o_in.at[n - 1], osend, orecv.at[n - 1], dev),
             remote(s_out.at[n - 1], s_in.at[n - 1], ssend, srecv.at[n - 1], dev),
@@ -306,43 +324,42 @@
 
     spread(0)
     z_copy(1).start()
-    ask(1)
     z_copy(2).start()
     z_copy(3).start()
+    pl.semaphore_wait(hello.at[2], 2)
+    ask(2)
+    ask(1)
     ask(3)
     pad_query(0, q_out[...])
     forward(0)
     spread(1)
-    pl.semaphore_wait(hello.at[2], 2)
-    ask(2)
     spread(2)
     complete(0)
+    forward(1)
+    block((0, 0))
     spread(3)
-    forward(1)
-    own(0)
-    forward(2)
+    arrive(2)
+    two_groups((2, 0))
     arrive(1)
     arrive(3)
     group_is(0, (1, 0), (3, 0))
-    forward(3)
+    group_is(1, (1, 0))
     complete(1)
-    group_is(0, (1, 1), (3, 1))
-    near_groups(1, (1, 0), (1, 1))
-    arrive(2)
+    group_is(0, (2, 1), (1, 1), (3, 1))
+    group_is(1, (2, 1), (1, 1))
+    group_is(2, (1, 0), (1, 1))
     complete(2)
-    two_groups((2, 0), (2, 1), (2, 2))
+    group_is(0, (2, 2), (1, 2), (3, 2))
+    group_is(1, (2, 2), (1, 2))
     complete(3)
-    group_is(0, (2, 3), (1, 2), (3, 2))
-    group_is(1, (2, 3), (1, 2))
+    two_groups((2, 3))
     give_back(2)
     group_is(0, (1, 3), (3, 3))
     give_back(3)
     group_is(1, (1, 3))
     group_is(2, (1, 2), (1, 3))
     give_back(1)
-    own(1)
-    own(2)
-    own(3)
+    own_rest()
 
     settle(three_halves, wrecv)
     for yy in (y_dn, y_up, y_far):
@@ -417,7 +434,7 @@
             v((3, HEAD_DIM, 256), BF16), v((3, 1, 256), F32),
             v((HEAD_DIM, 256), F32), v((8, 256), F32),
             v((8, 32, 128), BF16), v((8, 32, 128), BF16),
-            dma((5,)), dma, dma((2, 2)), dma((2,)), dma, dma, dma, dma((3,)),
+            dma((5,)), dma, dma((2, 3)), dma((2, 2)), dma, dma, dma, dma((3,)),
             dma, dma((3,)), dma, dma((2, 4)), dma((4,)),
             dma, dma((3,)), dma, dma((3,)),
             dma, dma, dma, dma, dma, dma, pltpu.SemaphoreType.REGULAR((3,)),

time: 49.8 us -> 49.4 us (level); the launches traced: 48.9 us -> 49.3 us
  no operation moved by 1% of the time
where the time goes in v5:
time: 49.4 us; the launch traced here: 49.3 us
  Pallas kernels  47.7 us (97%)
  local copies, waits for them, and re-layouts  1.57 us (3%)
    pallas_call x1, Pallas kernels, per_device(): pl.pallas_call(layer_kernel, out_shape=jax.ShapeDtypeStruct((32, 2048), B...  47.7 us
    unnamed x1, local copies, waits for them, and re-layouts  1.57 us

profile of v5, /device:TPU:1, one launch (start us, length us, event | category | flops | bytes accessed | tf_op | source)
XLA Modules:
  0.0 49.3 jit_solution(9690401809682601990)
XLA Ops:
  0.0 47.7 %shard_map.73 = bf16[32,2048]{1,0:T(8,128)(2,1)} custom-call(bf16[2,16,2048]{2,1,0:T(8,128)(2,1)} %bitcast.4, f32[1,2048]{1,0:T(1,128)} %bitcast.5, f32[2]{0:T(128)} %off_hbm.1, bf16[2048,128]{1,0:T(8,128)(2,1)} %wq_hbm.1, bf16[2048,128]{1,0:T(8,128)(2,1)} %wk_hbm.1, bf16[2048,128]{1,0:T(8,128)(2,1)} %wv_hbm.1, bf16[2,64,2048]{2,1,0:T(8,128)(2,1)} %bitcast.3), custom_call_target="tpu_custom_call" | custom-call | tf_op jit(solution)/shard_map/pallas_call | solution.py:419
  47.7 1.6 %copy.9 = bf16[32,2048]{1,0:T(8,128)(2,1)} copy(bf16[32,2048]{1,0:T(8,128)(2,1)} %shard_map.73) | data formatting | bytes 262144

commit v6 on v5

--- a/solution.py
+++ b/solution.py
@@ -68,17 +68,41 @@
     y_up, y_dn, y_far = (y + 1) % 4, (y + 3) % 4, (y + 2) % 4
     peers = (at(z, x, c, y_up), at(z, x, c, y_dn))
 
-    def greet(sem, devs):
-        for dev in devs:
-            pl.semaphore_signal(sem, inc=1, device_id=dev, device_id_type=MESH)
-        pl.semaphore_wait(sem, len(devs))
-
-    def along_z(n):
-        return [at((z + n) % 16, x, c, y), at((z + 16 - n) % 16, x, c, y)]
-
     partner = at(z, x, 1 - c, y)
     sides = [at(z, (x + 1) % 4, c, y), at(z, (x + 3) % 4, c, y)]
-    greet(pltpu.get_barrier_semaphore(), [*peers, partner, *sides, *along_z(1)])
+    below = {1: (z + 12) % 16, 2: (z + 27 - 2 * r) % 16, 3: (z + 4) % 16}
+    above = {1: (z + 4) % 16, 2: (z + 27 - 2 * r) % 16, 3: (z + 12) % 16}
+
+    def tell(sem, dev):
+        pl.semaphore_signal(sem, inc=1, device_id=dev, device_id_type=MESH)
+
+    def greet(sem, devs, step):
+        for dev in devs:
+            tell(sem, dev)
+
+        @pl.when(z >= step)
+        def _():
+            tell(sem, at(z - step, x, c, y))
+
+        @pl.when(z + step <= 15)
+        def _():
+            tell(sem, at(z + step, x, c, y))
+
+        return len(devs) + jnp.where(z >= step, 1, 0) + jnp.where(z + step <= 15, 1, 0)
+
+    barrier = pltpu.get_barrier_semaphore()
+    count = greet(barrier, [*peers, partner, *sides], 1)
+
+    @pl.when(group == 0)
+    def _():
+        tell(barrier, at(above[3], x, c, y))
+
+    @pl.when(jnp.logical_and(group < 2, r < 2))
+    def _():
+        tell(barrier, at(above[2], x, c, y))
+
+    count = count + jnp.where(group == 3, 1, 0) + jnp.where(jnp.logical_and(group >= 2, r >= 2), 1, 0)
+    pl.semaphore_wait(barrier, count)
     for cp in early:
         cp.wait()
     cols = (pl.ds(0, 1024), pl.ds(1024, 1024))
@@ -93,7 +117,7 @@
     for cp in first.values():
         cp.start()
 
-    greet(hello.at[0], [*peers, partner, *sides, *along_z(1)])
+    pl.semaphore_wait(hello.at[0], greet(hello.at[0], [*peers, partner, *sides], 1))
     gain = gain_ref[...]
 
     def norm_rows(rows):
@@ -115,9 +139,8 @@
             piece = tok_all.at[(y_dn, y_up)[d], d, :, cols[n]]
             relays.append(remote(piece, piece, ysend, y2recv.at[d, n], peers[d]))
             relays[-1].start()
-    greet(hello.at[1], [partner, *along_z(2)])
-    for dev in along_z(4):
-        pl.semaphore_signal(hello.at[2], inc=1, device_id=dev, device_id_type=MESH)
+    pl.semaphore_wait(hello.at[1], greet(hello.at[1], [partner], 2))
+    told = greet(hello.at[2], [], 4)
     q_pad[...] = jnp.zeros((4, 256, 128), BF16)
     normed[y_dn, pl.ds(0, 16), :] = norm_rows(tok_all[y_dn, 0])
     normed[y_up, pl.ds(16, 16), :] = norm_rows(tok_all[y_up, 1])
@@ -157,9 +180,6 @@
     kv_sib = sib_in[0]
     pair = jnp.concatenate([jnp.where(mine0, kv_mine, kv_sib), jnp.where(mine0, kv_sib, kv_mine)], axis=0)
     kv_all[r, x] = dot(perm, pair).astype(BF16)
-
-    below = {1: (z + 12) % 16, 2: (z + 27 - 2 * r) % 16, 3: (z + 4) % 16}
-    above = {1: (z + 4) % 16, 2: (z + 27 - 2 * r) % 16, 3: (z + 12) % 16}
 
     def q_copy(n):
         return remote(q_out, q_in.at[n - 1], qsend, qrecv.at[n - 1], at(below[n], x, c, y))
@@ -326,13 +346,13 @@
     z_copy(1).start()
     z_copy(2).start()
     z_copy(3).start()
-    pl.semaphore_wait(hello.at[2], 2)
+    pl.semaphore_wait(hello.at[2], told)
     ask(2)
-    ask(1)
-    ask(3)
     pad_query(0, q_out[...])
     forward(0)
     spread(1)
+    ask(1)
+    ask(3)
     spread(2)
     complete(0)
     forward(1)

time: 49.4 us -> 48.9 us (0.990)
  the two profiles are of different devices: /device:TPU:1 before, /device:TPU:385 now
where the time goes in v6:
time: 48.9 us; the launch traced here: 48.7 us
  Pallas kernels  47.1 us (96%)
  local copies, waits for them, and re-layouts  1.57 us (3%)
    pallas_call x1, Pallas kernels, per_device(): pl.pallas_call(layer_kernel, out_shape=jax.ShapeDtypeStruct((32, 2048), B...  47.1 us
    unnamed x1, local copies, waits for them, and re-layouts  1.57 us

profile of v6, /device:TPU:385, one launch (start us, length us, event | category | flops | bytes accessed | tf_op | source)
XLA Modules:
  0.0 48.7 jit_solution(734416051870244397)
XLA Ops:
  0.0 47.1 %shard_map.73 = bf16[32,2048]{1,0:T(8,128)(2,1)} custom-call(bf16[2,16,2048]{2,1,0:T(8,128)(2,1)} %bitcast.4, f32[1,2048]{1,0:T(1,128)} %bitcast.5, f32[2]{0:T(128)} %off_hbm.1, bf16[2048,128]{1,0:T(8,128)(2,1)} %wq_hbm.1, bf16[2048,128]{1,0:T(8,128)(2,1)} %wk_hbm.1, bf16[2048,128]{1,0:T(8,128)(2,1)} %wv_hbm.1, bf16[2,64,2048]{2,1,0:T(8,128)(2,1)} %bitcast.3), custom_call_target="tpu_custom_call" | custom-call | tf_op jit(solution)/shard_map/pallas_call | solution.py:439
  47.2 1.6 %copy.9 = bf16[32,2048]{1,0:T(8,128)(2,1)} copy(bf16[32,2048]{1,0:T(8,128)(2,1)} %shard_map.73) | data formatting | bytes 262144
